TPU v7x, 32 devices: a whole 2x2x4 slice. The times are simulated.
32 devices in a mesh: ep: 8 (over z, x), tp: 4 (over y, core).
Axes of the slice: x: 2, y: 2, z: 4, core: 2. Of those that a mesh axis runs over, the one named last changes fastest.
Arguments:
- receptance: bfloat16 [4096, 1024], P('ep', 'tp'), may hold values from -6 to 6
- key_matrix: bfloat16 [4096, 1024], P('ep', 'tp'), may hold values from -6 to 6
- value_matrix: bfloat16 [4096, 1024], P('ep', 'tp'), may hold values from -6 to 6
- decay_data_term: bfloat16 [4096, 1024], P('ep', 'tp'), may hold values from -3.5 to 3.5
- correction_rate_data: bfloat16 [4096, 1024], P('ep', 'tp'), may hold values from -6 to 6
- output_gate_input: bfloat16 [4096, 1024], P('ep', 'tp'), may hold values from -6 to 6
- decay_channel_offset: float32 [1024], P('tp'), may hold values from -12 to -2
- correction_rate_offset: float32 [1024], P('tp'), may hold values from -12 to 1
- extra_head_log_decay: float32 [4096, 16], P('ep', 'tp'), may hold values from -2.1 to 0, as said below
- head_norm_gain: float32 [1024], P('tp'), may hold values from 0.1 to 1.9
- mixer_output_weight: bfloat16 [1024, 2048], P('tp'), may hold values from -0.1875 to 0.1875
- expert_layer_input: bfloat16 [1024, 2048], P('ep'), may hold values from -6 to 6
- feedforward_norm_gain: float32 [2048], replicated, may hold values from 0.1 to 1.9
- group_router_weight: bfloat16 [2048, 4], replicated, may hold values from -0.125 to 0.125
- expert_router_weight: bfloat16 [2048, 8], replicated, may hold values from -0.125 to 0.125
- routes: int32 [1024, 2], P('ep'), may hold values from 0 to 7, all different within a row; in each aligned block of 128 rows (0 to 127, 128 to 255, ...) at most 64 rows name the same one
- expert_gate_weight: bfloat16 [8, 2048, 4096], P('ep', None, 'tp'), may hold values from -0.125 to 0.125
- expert_up_weight: bfloat16 [8, 2048, 4096], P('ep', None, 'tp'), may hold values from -0.125 to 0.125
- expert_down_weight: bfloat16 [8, 4096, 2048], P('ep', 'tp'), may hold values from -0.09375 to 0.09375
Outputs:
- token_mixer_output: bfloat16 [4096, 2048], P(('ep', 'tp'))
- expert_out: bfloat16 [1024, 2048], P('ep', 'tp')
Inputs may be any that keep to these rules, and one draw needn't show every extreme that they name: A token's routes are distinct. Within the rows of one index of ep, no expert is named by more than 64 rows, a bound that some block reaches. `extra_head_log_decay`: entries are zero or negative; each head has a few nonzero positions.
All inputs are finite; a program needn't handle non-finite values.
Results may differ from a plain program's by a relative error of at most 0.022.
Values may be sent and summed in bfloat16 or wider, within the bound.
A program may use at most 128 MiB of HBM per device.

v0:
```python
import jax
import jax.numpy as jnp
from jax import lax
from jax.sharding import PartitionSpec as P

HEAD_DIM = 64
GROUPS = 4


key_eps = 1e-06
group_eps = 0.00064
norm_eps = 1e-06
highest = lax.Precision.HIGHEST


def carried_in(value, axis, combine, identity):
    devices, place = (lax.axis_size(axis), lax.axis_index(axis))
    everything = jax.tree.map(
        lambda part, kind: lax.all_gather(part.astype(kind), axis),
        value,
        (jnp.bfloat16, jnp.bfloat16),
    )
    start = jax.tree.map(
        lambda part, zero: jnp.broadcast_to(jnp.asarray(zero, part.dtype), part.shape),
        value,
        identity,
    )

    def hop(k, before):
        reached = k < place
        new = combine(
            before, jax.tree.map(lambda part, own: part[k].astype(own.dtype), everything, value)
        )
        return jax.tree.map(lambda a, b: jnp.where(reached, a, b), new, before)

    return lax.fori_loop(0, devices, hop, start)


def chain_join(earlier, later):
    joined_map = jnp.einsum("hvk,hkj->hvj", earlier[0], later[0], precision=highest)
    joined_state = jnp.einsum("hvk,hkj->hvj", earlier[1], later[0], precision=highest) + later[1]
    return (joined_map, joined_state)


def pair_decay(upper, lower, keep):
    gap = upper[:, None] - lower[None, :]
    mask = keep[:, :, None, None]
    return jnp.where(mask, jnp.exp(jnp.where(mask, gap, 0.0)), 0.0)


def block_advance(stacked, inputs):
    recept_b, log_b, unit_b, removal_b, key_b, value_b = inputs
    block_len = recept_b.shape[0]
    cumul = jnp.cumsum(log_b, axis=0)
    before = cumul - log_b
    places = jnp.arange(block_len)
    strict = places[:, None] > places[None, :]
    upto = places[:, None] >= places[None, :]
    strict_decay = pair_decay(before, cumul, strict)
    upto_decay = pair_decay(cumul, cumul, upto)
    key_pairs = jnp.einsum("jhk,ihk,jihk->hji", unit_b, key_b, strict_decay, precision=highest)
    removal_pairs = jnp.einsum(
        "jhk,ihk,jihk->hji", unit_b, removal_b, strict_decay, precision=highest
    )
    read_keys = jnp.einsum("thk,ihk,tihk->hti", recept_b, key_b, upto_decay, precision=highest)
    read_removal = jnp.einsum(
        "thk,ihk,tihk->hti", recept_b, removal_b, upto_decay, precision=highest
    )
    value_padded = jnp.concatenate([value_b, jnp.zeros_like(value_b)], axis=-1)
    right_side = jnp.einsum(
        "jhk,hrk->hjr", unit_b * jnp.exp(before), stacked, precision=highest
    ) + jnp.einsum("hji,ihr->hjr", key_pairs, value_padded, precision=highest)
    left_side = jnp.eye(block_len, dtype=jnp.float32)[None] + removal_pairs
    corrected = jax.scipy.linalg.solve_triangular(
        left_side, right_side, lower=True, unit_diagonal=True
    )
    outputs = (
        jnp.einsum("thk,hrk->thr", recept_b * jnp.exp(cumul), stacked, precision=highest)
        + jnp.einsum("hti,ihr->thr", read_keys, value_padded, precision=highest)
        - jnp.einsum("hti,hir->thr", read_removal, corrected, precision=highest)
    )
    tail = jnp.exp(cumul[-1][None] - cumul)
    stacked = (
        stacked * jnp.exp(cumul[-1])[:, None, :]
        + jnp.einsum("ihr,ihk->hrk", value_padded, key_b * tail, precision=highest)
        - jnp.einsum("hir,ihk->hrk", corrected, removal_b * tail, precision=highest)
    )
    return (stacked, outputs)


def mixer_part(
    receptance,
    key_matrix,
    value_matrix,
    decay_data_term,
    correction_rate_data,
    output_gate_input,
    decay_channel_offset,
    correction_rate_offset,
    extra_head_log_decay,
    head_norm_gain,
    mixer_output_weight,
):
    positions = receptance.shape[0]
    head_count = receptance.shape[1] // HEAD_DIM

    def head_view(tensor_in):
        return tensor_in.astype(jnp.float32).reshape(positions, head_count, HEAD_DIM)

    recept = head_view(receptance)
    keyed = head_view(key_matrix)
    valued = head_view(value_matrix)
    unit_keys = keyed * lax.rsqrt(jnp.sum(keyed * keyed, axis=-1, keepdims=True) + key_eps)
    learn_rate = jax.nn.sigmoid(
        head_view(correction_rate_data) + correction_rate_offset.reshape(head_count, HEAD_DIM)
    )
    decay_preactivation = head_view(decay_data_term) + decay_channel_offset.reshape(
        head_count, HEAD_DIM
    )
    decay_logarithm = (
        -jnp.exp(-jax.nn.softplus(-decay_preactivation) - 0.5) + extra_head_log_decay[:, :, None]
    )
    removal = unit_keys * learn_rate
    block_len = min(64, positions)
    block_count = positions // block_len

    def blocked(tensor_in):
        return tensor_in.reshape(block_count, block_len, head_count, HEAD_DIM)

    eye_maps = jnp.broadcast_to(
        jnp.eye(HEAD_DIM, dtype=jnp.float32), (head_count, HEAD_DIM, HEAD_DIM)
    )
    zero_state = jnp.zeros((head_count, HEAD_DIM, HEAD_DIM), jnp.float32)
    start = jnp.concatenate([zero_state, eye_maps], axis=1)
    final, outputs = lax.scan(
        block_advance,
        start,
        (
            blocked(recept),
            blocked(decay_logarithm),
            blocked(unit_keys),
            blocked(removal),
            blocked(keyed),
            blocked(valued),
        ),
    )
    outputs = outputs.reshape(positions, head_count, 2 * HEAD_DIM)
    local_read = outputs[:, :, :HEAD_DIM]
    reached = outputs[:, :, HEAD_DIM:]
    state_end = final[:, :HEAD_DIM]
    transfer_end = final[:, HEAD_DIM:]
    prefix = carried_in((transfer_end, state_end), "ep", chain_join, (eye_maps, zero_state))
    head_out = local_read + jnp.einsum("hvk,thk->thv", prefix[1], reached, precision=highest)
    centre = jnp.mean(head_out, axis=-1, keepdims=True)
    spread = jnp.mean(jnp.square(head_out - centre), axis=-1, keepdims=True)
    normed = (head_out - centre) * lax.rsqrt(spread + group_eps)
    gated = (
        normed
        * head_norm_gain.reshape(head_count, HEAD_DIM)
        * jax.nn.sigmoid(head_view(output_gate_input))
    )
    mixed_hidden = gated.reshape(positions, head_count * HEAD_DIM).astype(jnp.bfloat16)
    return lax.psum_scatter(
        jnp.dot(mixed_hidden, mixer_output_weight, preferred_element_type=jnp.float32).astype(
            jnp.bfloat16
        ),
        "tp",
        scatter_dimension=0,
        tiled=True,
    )


def finish_experts(gate_val, up_val, expert_down_weight):
    expert_hidden = (jax.nn.silu(gate_val) * up_val).astype(jnp.bfloat16)
    return lax.psum_scatter(
        jnp.einsum(
            "sxcf,xfd->dsxc", expert_hidden, expert_down_weight, preferred_element_type=jnp.float32
        ).astype(jnp.bfloat16),
        "tp",
        scatter_dimension=0,
        tiled=True,
    )


def expert_part(
    expert_layer_input,
    feedforward_norm_gain,
    group_router_weight,
    expert_router_weight,
    routes,
    expert_gate_weight,
    expert_up_weight,
    expert_down_weight,
):
    token_rows = expert_layer_input.shape[0]
    route_count = routes.shape[1]
    ep_count = lax.axis_size("ep")
    expert_total = expert_router_weight.shape[1]
    per_group = expert_total // GROUPS
    capacity = 4 * token_rows // ep_count
    widened = expert_layer_input.astype(jnp.float32)
    normed_input = (
        widened
        * lax.rsqrt(jnp.mean(widened * widened, axis=-1, keepdims=True) + norm_eps)
        * feedforward_norm_gain
    ).astype(jnp.bfloat16)
    group_logit = jnp.dot(normed_input, group_router_weight, preferred_element_type=jnp.float32)
    group_exp = jnp.exp(group_logit)
    group_prob = group_exp / jnp.sum(group_exp, axis=-1, keepdims=True)
    expert_logit = jnp.dot(normed_input, expert_router_weight, preferred_element_type=jnp.float32)
    expert_range = jnp.arange(expert_total, dtype=jnp.int32)
    matched = routes[:, :, None] == expert_range[None, None, :]
    chosen_logit = jnp.sum(jnp.where(matched, expert_logit[:, None, :], 0.0), axis=-1)
    group_match = (routes // per_group)[:, :, None] == jnp.arange(GROUPS, dtype=jnp.int32)[
        None, None, :
    ]
    chosen_group = jnp.sum(jnp.where(group_match, group_prob[:, None, :], 0.0), axis=-1)
    route_weight = chosen_group * jax.nn.sigmoid(chosen_logit - chosen_logit[:, ::-1])
    flat_match = matched.reshape(token_rows * route_count, expert_total).astype(jnp.int32)
    before = jnp.cumsum(flat_match, axis=0) - flat_match
    placed = jnp.sum(before * flat_match, axis=1)
    slot_ids = routes.reshape(-1) * capacity + placed
    slot_range = jnp.arange(expert_total * capacity, dtype=jnp.int32)
    struck = (slot_range[:, None] == slot_ids[None, :]).reshape(
        expert_total * capacity, token_rows, route_count
    )
    dispatch_matrix = jnp.any(struck, axis=-1).astype(jnp.bfloat16)
    combine_matrix = jnp.sum(jnp.where(struck, route_weight[None, :, :], 0.0), axis=-1)
    outgoing = jnp.dot(dispatch_matrix, normed_input, preferred_element_type=jnp.float32).astype(
        jnp.bfloat16
    )
    outgoing = outgoing.reshape(ep_count, expert_total // ep_count, capacity, outgoing.shape[1])
    width_share = outgoing.shape[3] // lax.axis_size("tp")
    own_columns = lax.dynamic_slice_in_dim(
        outgoing, lax.axis_index("tp") * width_share, width_share, 3
    )
    piece = lax.all_gather(
        lax.all_to_all(own_columns, "ep", split_axis=0, concat_axis=0, tiled=True),
        "tp",
        axis=3,
        tiled=True,
    )
    gate_val = jnp.einsum(
        "sxcd,xdf->sxcf", piece, expert_gate_weight, preferred_element_type=jnp.float32
    )
    up_val = jnp.einsum(
        "sxcd,xdf->sxcf", piece, expert_up_weight, preferred_element_type=jnp.float32
    )
    expert_rows = finish_experts(gate_val, up_val, expert_down_weight)
    homebound = lax.all_to_all(expert_rows, "ep", split_axis=1, concat_axis=1, tiled=True)
    homebound = homebound.reshape(homebound.shape[0], expert_total * capacity)
    combined = jnp.dot(homebound.astype(jnp.float32), combine_matrix, precision=highest)
    return combined.T.astype(jnp.bfloat16)


def local(
    receptance,
    key_matrix,
    value_matrix,
    decay_data_term,
    correction_rate_data,
    output_gate_input,
    decay_channel_offset,
    correction_rate_offset,
    extra_head_log_decay,
    head_norm_gain,
    mixer_output_weight,
    expert_layer_input,
    feedforward_norm_gain,
    group_router_weight,
    expert_router_weight,
    routes,
    expert_gate_weight,
    expert_up_weight,
    expert_down_weight,
):
    token_mixer_output = mixer_part(
        receptance,
        key_matrix,
        value_matrix,
        decay_data_term,
        correction_rate_data,
        output_gate_input,
        decay_channel_offset,
        correction_rate_offset,
        extra_head_log_decay,
        head_norm_gain,
        mixer_output_weight,
    )
    expert_out = expert_part(
        expert_layer_input,
        feedforward_norm_gain,
        group_router_weight,
        expert_router_weight,
        routes,
        expert_gate_weight,
        expert_up_weight,
        expert_down_weight,
    )
    return (token_mixer_output, expert_out)


def solution(mesh):
    in_specs = (
        P("ep", "tp"),
        P("ep", "tp"),
        P("ep", "tp"),
        P("ep", "tp"),
        P("ep", "tp"),
        P("ep", "tp"),
        P("tp"),
        P("tp"),
        P("ep", "tp"),
        P("tp"),
        P("tp", None),
        P("ep", None),
        P(),
        P(),
        P(),
        P("ep", None),
        P("ep", None, "tp"),
        P("ep", None, "tp"),
        P("ep", "tp", None),
    )
    out_specs = (P(("ep", "tp"), None), P("ep", "tp"))
    return jax.shard_map(local, mesh=mesh, in_specs=in_specs, out_specs=out_specs, check_vma=False)
```

profile of v0, /device:TPU:0, one launch (start us, length us, event | category | flops | bytes accessed | tf_op | source)
XLA Modules:
  0.0 763.8 jit_solution(9080496010554632357)
XLA Ops:
  37.6 566.0 %while.26 = (s32[]{:T(128)}, f32[4,128,64]{1,2,0:T(8,128)S(1)}, f32[8,64,4,128]{3,1,0,2:T(8,128)}, f32[8,64,4,64]{3,2,1,0:T(4,128)}, f32[8,64,4,64]{3,2,1,0:T(4,...) while((s32[]{:T(128)}, f32[4,128,64]{1,2,0:T(8,128)S(1)}, ...), condition=%wide.region_3.4_spmd, body=%wide.region_1.3_spmd.sunk | while | flops 221540416 | bytes 39878260 | solution.py:135
  40.0 12.8 %select_bitcast_fusion.3 = (f32[4,64,64,64]{3,0,2,1:T(4,128)}, f32[4,64,64,64]{3,0,2,1:T(4,128)}) fusion(f32[64,4,64]{2,1,0:T(4,128)S(1)} %fusion.151, pred[64,64]{1,0:T(8,128)(4,1)S(1)} %get-tuple-element.380, f32[64,4,64]{2,1,0:T(4,128)S(1)} %get-tuple-element.381, pred[64,64]{1,0:T(8,128)(4,1)S(1)} %get-tuple-element.382), kind=kLoop, calls=%fused_computation.19.clone.1 | loop fusion | flops 6291456 | bytes 8527872 | tf_op jit(solution)/shard_map/while
  52.8 10.7 %copy.249 = f32[4,64,64,64]{1,2,3,0:T(8,128)} copy(f32[4,64,64,64]{3,0,2,1:T(4,128)} %get-tuple-element.383) | data formatting | bytes 8388608 | tf_op jit(solution)/shard_map/while
  63.5 10.6 %copy.253 = f32[4,64,64,64]{1,2,3,0:T(8,128)} copy(f32[4,64,64,64]{3,0,2,1:T(4,128)} %get-tuple-element.387) | data formatting | bytes 8388608 | tf_op jit(solution)/shard_map/while
  76.6 7.5 fusion.154
  84.3 19.7 %custom-call.7 = f32[4,1,64,64]{2,3,1,0:T(8,128)S(1)} custom-call(f32[4,1,64,64]{3,2,1,0:T(8,128)S(1)} %add_bitcast_fusion.2), custom_call_target="InvertDiagBlocksLowerTriangular" | custom-call | tf_op jit(solution)/shard_map/while/body/eval_jaxpr/jit(_solve_triangular)/vmap()/triangular_solve | solution.py:74
  110.8 12.8 %select_bitcast_fusion.3 = (f32[4,64,64,64]{3,0,2,1:T(4,128)}, f32[4,64,64,64]{3,0,2,1:T(4,128)}) fusion(f32[64,4,64]{2,1,0:T(4,128)S(1)} %fusion.151, pred[64,64]{1,0:T(8,128)(4,1)S(1)} %get-tuple-element.380, f32[64,4,64]{2,1,0:T(4,128)S(1)} %get-tuple-element.381, pred[64,64]{1,0:T(8,128)(4,1)S(1)} %get-tuple-element.382), kind=kLoop, calls=%fused_computation.19.clone.1 | loop fusion | flops 6291456 | bytes 8527872 | tf_op jit(solution)/shard_map/while
  123.6 10.7 %copy.249 = f32[4,64,64,64]{1,2,3,0:T(8,128)} copy(f32[4,64,64,64]{3,0,2,1:T(4,128)} %get-tuple-element.383) | data formatting | bytes 8388608 | tf_op jit(solution)/shard_map/while
  134.2 10.6 %copy.253 = f32[4,64,64,64]{1,2,3,0:T(8,128)} copy(f32[4,64,64,64]{3,0,2,1:T(4,128)} %get-tuple-element.387) | data formatting | bytes 8388608 | tf_op jit(solution)/shard_map/while
  147.3 7.5 fusion.154
  155.0 19.7 %custom-call.7 = f32[4,1,64,64]{2,3,1,0:T(8,128)S(1)} custom-call(f32[4,1,64,64]{3,2,1,0:T(8,128)S(1)} %add_bitcast_fusion.2), custom_call_target="InvertDiagBlocksLowerTriangular" | custom-call | tf_op jit(solution)/shard_map/while/body/eval_jaxpr/jit(_solve_triangular)/vmap()/triangular_solve | solution.py:74
  181.5 12.8 %select_bitcast_fusion.3 = (f32[4,64,64,64]{3,0,2,1:T(4,128)}, f32[4,64,64,64]{3,0,2,1:T(4,128)}) fusion(f32[64,4,64]{2,1,0:T(4,128)S(1)} %fusion.151, pred[64,64]{1,0:T(8,128)(4,1)S(1)} %get-tuple-element.380, f32[64,4,64]{2,1,0:T(4,128)S(1)} %get-tuple-element.381, pred[64,64]{1,0:T(8,128)(4,1)S(1)} %get-tuple-element.382), kind=kLoop, calls=%fused_computation.19.clone.1 | loop fusion | flops 6291456 | bytes 8527872 | tf_op jit(solution)/shard_map/while
  194.3 10.7 %copy.249 = f32[4,64,64,64]{1,2,3,0:T(8,128)} copy(f32[4,64,64,64]{3,0,2,1:T(4,128)} %get-tuple-element.383) | data formatting | bytes 8388608 | tf_op jit(solution)/shard_map/while
  205.0 10.6 %copy.253 = f32[4,64,64,64]{1,2,3,0:T(8,128)} copy(f32[4,64,64,64]{3,0,2,1:T(4,128)} %get-tuple-element.387) | data formatting | bytes 8388608 | tf_op jit(solution)/shard_map/while
  218.0 7.5 fusion.154
  225.7 19.7 %custom-call.7 = f32[4,1,64,64]{2,3,1,0:T(8,128)S(1)} custom-call(f32[4,1,64,64]{3,2,1,0:T(8,128)S(1)} %add_bitcast_fusion.2), custom_call_target="InvertDiagBlocksLowerTriangular" | custom-call | tf_op jit(solution)/shard_map/while/body/eval_jaxpr/jit(_solve_triangular)/vmap()/triangular_solve | solution.py:74
  252.3 12.8 %select_bitcast_fusion.3 = (f32[4,64,64,64]{3,0,2,1:T(4,128)}, f32[4,64,64,64]{3,0,2,1:T(4,128)}) fusion(f32[64,4,64]{2,1,0:T(4,128)S(1)} %fusion.151, pred[64,64]{1,0:T(8,128)(4,1)S(1)} %get-tuple-element.380, f32[64,4,64]{2,1,0:T(4,128)S(1)} %get-tuple-element.381, pred[64,64]{1,0:T(8,128)(4,1)S(1)} %get-tuple-element.382), kind=kLoop, calls=%fused_computation.19.clone.1 | loop fusion | flops 6291456 | bytes 8527872 | tf_op jit(solution)/shard_map/while
  265.1 10.7 %copy.249 = f32[4,64,64,64]{1,2,3,0:T(8,128)} copy(f32[4,64,64,64]{3,0,2,1:T(4,128)} %get-tuple-element.383) | data formatting | bytes 8388608 | tf_op jit(solution)/shard_map/while
  275.7 10.6 %copy.253 = f32[4,64,64,64]{1,2,3,0:T(8,128)} copy(f32[4,64,64,64]{3,0,2,1:T(4,128)} %get-tuple-element.387) | data formatting | bytes 8388608 | tf_op jit(solution)/shard_map/while
  288.8 7.5 fusion.154
  296.5 19.7 %custom-call.7 = f32[4,1,64,64]{2,3,1,0:T(8,128)S(1)} custom-call(f32[4,1,64,64]{3,2,1,0:T(8,128)S(1)} %add_bitcast_fusion.2), custom_call_target="InvertDiagBlocksLowerTriangular" | custom-call | tf_op jit(solution)/shard_map/while/body/eval_jaxpr/jit(_solve_triangular)/vmap()/triangular_solve | solution.py:74
  323.0 12.8 %select_bitcast_fusion.3 = (f32[4,64,64,64]{3,0,2,1:T(4,128)}, f32[4,64,64,64]{3,0,2,1:T(4,128)}) fusion(f32[64,4,64]{2,1,0:T(4,128)S(1)} %fusion.151, pred[64,64]{1,0:T(8,128)(4,1)S(1)} %get-tuple-element.380, f32[64,4,64]{2,1,0:T(4,128)S(1)} %get-tuple-element.381, pred[64,64]{1,0:T(8,128)(4,1)S(1)} %get-tuple-element.382), kind=kLoop, calls=%fused_computation.19.clone.1 | loop fusion | flops 6291456 | bytes 8527872 | tf_op jit(solution)/shard_map/while
  335.8 10.7 %copy.249 = f32[4,64,64,64]{1,2,3,0:T(8,128)} copy(f32[4,64,64,64]{3,0,2,1:T(4,128)} %get-tuple-element.383) | data formatting | bytes 8388608 | tf_op jit(solution)/shard_map/while
  346.5 10.6 %copy.253 = f32[4,64,64,64]{1,2,3,0:T(8,128)} copy(f32[4,64,64,64]{3,0,2,1:T(4,128)} %get-tuple-element.387) | data formatting | bytes 8388608 | tf_op jit(solution)/shard_map/while
  359.5 7.5 fusion.154
  367.2 19.7 %custom-call.7 = f32[4,1,64,64]{2,3,1,0:T(8,128)S(1)} custom-call(f32[4,1,64,64]{3,2,1,0:T(8,128)S(1)} %add_bitcast_fusion.2), custom_call_target="InvertDiagBlocksLowerTriangular" | custom-call | tf_op jit(solution)/shard_map/while/body/eval_jaxpr/jit(_solve_triangular)/vmap()/triangular_solve | solution.py:74
  393.7 12.8 %select_bitcast_fusion.3 = (f32[4,64,64,64]{3,0,2,1:T(4,128)}, f32[4,64,64,64]{3,0,2,1:T(4,128)}) fusion(f32[64,4,64]{2,1,0:T(4,128)S(1)} %fusion.151, pred[64,64]{1,0:T(8,128)(4,1)S(1)} %get-tuple-element.380, f32[64,4,64]{2,1,0:T(4,128)S(1)} %get-tuple-element.381, pred[64,64]{1,0:T(8,128)(4,1)S(1)} %get-tuple-element.382), kind=kLoop, calls=%fused_computation.19.clone.1 | loop fusion | flops 6291456 | bytes 8527872 | tf_op jit(solution)/shard_map/while
  406.5 10.7 %copy.249 = f32[4,64,64,64]{1,2,3,0:T(8,128)} copy(f32[4,64,64,64]{3,0,2,1:T(4,128)} %get-tuple-element.383) | data formatting | bytes 8388608 | tf_op jit(solution)/shard_map/while
  417.2 10.6 %copy.253 = f32[4,64,64,64]{1,2,3,0:T(8,128)} copy(f32[4,64,64,64]{3,0,2,1:T(4,128)} %get-tuple-element.387) | data formatting | bytes 8388608 | tf_op jit(solution)/shard_map/while
  430.3 7.5 fusion.154
  438.0 19.7 %custom-call.7 = f32[4,1,64,64]{2,3,1,0:T(8,128)S(1)} custom-call(f32[4,1,64,64]{3,2,1,0:T(8,128)S(1)} %add_bitcast_fusion.2), custom_call_target="InvertDiagBlocksLowerTriangular" | custom-call | tf_op jit(solution)/shard_map/while/body/eval_jaxpr/jit(_solve_triangular)/vmap()/triangular_solve | solution.py:74
  464.5 12.8 %select_bitcast_fusion.3 = (f32[4,64,64,64]{3,0,2,1:T(4,128)}, f32[4,64,64,64]{3,0,2,1:T(4,128)}) fusion(f32[64,4,64]{2,1,0:T(4,128)S(1)} %fusion.151, pred[64,64]{1,0:T(8,128)(4,1)S(1)} %get-tuple-element.380, f32[64,4,64]{2,1,0:T(4,128)S(1)} %get-tuple-element.381, pred[64,64]{1,0:T(8,128)(4,1)S(1)} %get-tuple-element.382), kind=kLoop, calls=%fused_computation.19.clone.1 | loop fusion | flops 6291456 | bytes 8527872 | tf_op jit(solution)/shard_map/while
  477.3 10.7 %copy.249 = f32[4,64,64,64]{1,2,3,0:T(8,128)} copy(f32[4,64,64,64]{3,0,2,1:T(4,128)} %get-tuple-element.383) | data formatting | bytes 8388608 | tf_op jit(solution)/shard_map/while
  487.9 10.6 %copy.253 = f32[4,64,64,64]{1,2,3,0:T(8,128)} copy(f32[4,64,64,64]{3,0,2,1:T(4,128)} %get-tuple-element.387) | data formatting | bytes 8388608 | tf_op jit(solution)/shard_map/while
  501.0 7.5 fusion.154
  508.7 19.7 %custom-call.7 = f32[4,1,64,64]{2,3,1,0:T(8,128)S(1)} custom-call(f32[4,1,64,64]{3,2,1,0:T(8,128)S(1)} %add_bitcast_fusion.2), custom_call_target="InvertDiagBlocksLowerTriangular" | custom-call | tf_op jit(solution)/shard_map/while/body/eval_jaxpr/jit(_solve_triangular)/vmap()/triangular_solve | solution.py:74
  535.2 12.8 %select_bitcast_fusion.3 = (f32[4,64,64,64]{3,0,2,1:T(4,128)}, f32[4,64,64,64]{3,0,2,1:T(4,128)}) fusion(f32[64,4,64]{2,1,0:T(4,128)S(1)} %fusion.151, pred[64,64]{1,0:T(8,128)(4,1)S(1)} %get-tuple-element.380, f32[64,4,64]{2,1,0:T(4,128)S(1)} %get-tuple-element.381, pred[64,64]{1,0:T(8,128)(4,1)S(1)} %get-tuple-element.382), kind=kLoop, calls=%fused_computation.19.clone.1 | loop fusion | flops 6291456 | bytes 8527872 | tf_op jit(solution)/shard_map/while
  548.0 10.7 %copy.249 = f32[4,64,64,64]{1,2,3,0:T(8,128)} copy(f32[4,64,64,64]{3,0,2,1:T(4,128)} %get-tuple-element.383) | data formatting | bytes 8388608 | tf_op jit(solution)/shard_map/while
  558.7 10.6 %copy.253 = f32[4,64,64,64]{1,2,3,0:T(8,128)} copy(f32[4,64,64,64]{3,0,2,1:T(4,128)} %get-tuple-element.387) | data formatting | bytes 8388608 | tf_op jit(solution)/shard_map/while
  571.7 7.5 fusion.154
  579.4 19.7 %custom-call.7 = f32[4,1,64,64]{2,3,1,0:T(8,128)S(1)} custom-call(f32[4,1,64,64]{3,2,1,0:T(8,128)S(1)} %add_bitcast_fusion.2), custom_call_target="InvertDiagBlocksLowerTriangular" | custom-call | tf_op jit(solution)/shard_map/while/body/eval_jaxpr/jit(_solve_triangular)/vmap()/triangular_solve | solution.py:74
  605.8 33.9 %all-gather = bf16[32,64,64]{2,1,0:T(8,128)(2,1)} all-gather(bf16[4,64,64]{2,1,0:T(8,128)(2,1)S(1)} %get-tuple-element.270), channel_id=2, replica_groups=mesh['ep'=8,'tp'=4] {'ep'}, dimensions={0}, use_global_device_ids=true | all-gather | bytes 294912 | tf_op jit(solution)/shard_map/all_gather | solution.py:19
  639.7 33.5 %all-gather.1 = bf16[32,64,64]{2,1,0:T(8,128)(2,1)} all-gather(bf16[4,64,64]{2,1,0:T(8,128)(2,1)S(1)} %get-tuple-element.269), channel_id=3, replica_groups=mesh['ep'=8,'tp'=4] {'ep'}, dimensions={0}, use_global_device_ids=true | all-gather | bytes 294912 | tf_op jit(solution)/shard_map/all_gather | solution.py:19
  679.6 10.7 %fusion.46 = bf16[2048,8,1,64]{0,3,1,2:T(8,128)(2,1)} fusion(bf16[1,1024,2048]{2,1,0:T(8,128)(2,1)} %param.41, f32[8,64,1024]{2,1,0:T(8,128)} %fusion.39, bf16[1,2048,1024]{2,1,0:T(8,128)(2,1)} %param.39, bf16[8,1,64,2048]{3,2,0,1:T(8,128)(2,1)} %all-gather.4.cloned.1.call-done), kind=kOutput, calls=%fused_computation.81 | convolution fusion | flops 4299161600 | bytes 14680064 | tf_op jit(solution)/shard_map/sxcf,xfd->dsxc/dot_general | solution.py:176
  690.6 17.0 %while.27 = (s32[]{:T(128)}, f32[4,64,64]{1,2,0:T(8,128)S(1)}, s32[]{:T(128)}, bf16[8,4,64,64]{3,2,1,0:T(8,128)(2,1)}, bf16[8,4,64,64]{3,2,1,0:T(8,128)(2,1)}, /*index=5*/s32[]{:T(128)}, s32[]{:T(128)}) while((s32[]{:T(128)}, f32[4,64,64]{1,2,0:T(8,128)S(1)}, s32[]{:T(128)}, bf16[8,4,64,64]{3,2,1,0:T(8,128)(2,1)}, ...), condition=%wide.region_5.6_spmd.clone, body=%wide.region_4.5_spmd.clone.sunk | while | flops 12664836 | bytes 723043 | solution.py:36
  712.0 10.9 %reduce-scatter.5.cloned.1.call-done = bf16[512,8,1,64]{0,3,1,2:T(8,128)(2,1)} async-done(((bf16[2048,8,1,64]{0,3,1,2:T(8,128)(2,1)}), bf16[512,8,1,64]{0,3,1,2:T(8,128)(2,1)}) %reduce-scatter.5.cloned.1.call-update) | async-done | bytes 524304 | tf_op jit(solution)/shard_map/reduce_scatter | solution.py:175
  728.9 13.8 %all-to-all-done.1 = bf16[512,8,1,64]{0,3,2,1:T(8,128)(2,1)S(1)} async-done(((bf16[512,8,1,64]{0,3,2,1:T(8,128)(2,1)}), bf16[512,8,1,64]{0,3,2,1:T(8,128)(2,1)S(1)}, u32[]{:S(2)}, u32[]{:S(2)}) %all-to-all-start.1) | async-done | bytes 524320 | tf_op jit(solution)/shard_map/all_to_all | solution.py:250
  743.8 13.4 %reduce-scatter.3.cloned.1.call-done = bf16[128,2048]{1,0:T(8,128)(2,1)} async-done(((bf16[512,2048]{1,0:T(8,128)(2,1)}), bf16[128,2048]{1,0:T(8,128)(2,1)}) %reduce-scatter.3.cloned.1.call-update) | async-done | bytes 524304 | tf_op jit(solution)/shard_map/reduce_scatter | solution.py:163
  (340 shorter events, 141.7 us)
Async XLA Ops:
  7.2 702.3 %copy-start = (bf16[256,2048]{1,0:T(8,128)(2,1)S(1)}, bf16[256,2048]{1,0:T(8,128)(2,1)}, u32[]{:S(2)}) copy-start(bf16[256,2048]{1,0:T(8,128)(2,1)} %param.33) | copy-start | bytes 3145732
  7.2 14.6 %copy-start.5 = (bf16[512,256]{1,0:T(8,128)(2,1)S(1)}, bf16[512,256]{1,0:T(8,128)(2,1)}, u32[]{:S(2)}) copy-start(bf16[512,256]{1,0:T(8,128)(2,1)} %param.24) | copy-start | bytes 786436
  11.5 1.9 copy-start.12
  11.5 12.9 %copy-start.3 = (bf16[512,256]{1,0:T(8,128)(2,1)S(1)}, bf16[512,256]{1,0:T(8,128)(2,1)}, u32[]{:S(2)}) copy-start(bf16[512,256]{1,0:T(8,128)(2,1)} %param.26) | copy-start | bytes 786436
  14.3 12.0 %copy-start.8 = (f32[512,4]{0,1:T(4,128)S(1)}, f32[512,4]{0,1:T(4,128)}, u32[]{:S(2)}) copy-start(f32[512,4]{0,1:T(4,128)} %param.31) | copy-start | bytes 24580
  14.3 12.9 %copy-start.9 = (f32[256]{0:T(256)S(1)}, f32[256]{0:T(256)}, u32[]{:S(2)}) copy-start(f32[256]{0:T(256)} %param.29) | copy-start | bytes 3076
  14.3 13.0 %copy-start.10 = (f32[256]{0:T(256)S(1)}, f32[256]{0:T(256)}, u32[]{:S(2)}) copy-start(f32[256]{0:T(256)} %param.30) | copy-start | bytes 3076
  14.3 23.0 %all-to-all-start = ((bf16[8,1,64,512]{3,2,1,0:T(8,128)(2,1)}), bf16[8,1,64,512]{3,2,1,0:T(8,128)(2,1)}, u32[]{:S(2)}, u32[]{:S(2)}) async-start(bf16[8,1,64,512]{3,2,1,0:T(8,128)(2,1)} %constant_dynamic-slice_fusion.2), calls=%async_computation.1 | async-start | bytes 1048576 | tf_op jit(solution)/shard_map/all_to_all | solution.py:238
  21.7 651.5 %all-gather.4.cloned.1.call-start = ((), (), s32[]{:S(2)}) async-start(), calls=%async_computation.5 | async-start | bytes 2621440 | tf_op jit(solution)/shard_map/all_gather | solution.py:237
  37.4 685.6 %reduce-scatter.5.cloned.1.call-start = ((), (), s32[]{:S(2)}) async-start(), calls=%async_computation.6 | async-start | bytes 2621440 | tf_op jit(solution)/shard_map/reduce_scatter | solution.py:175
  37.6 567.7 %copy-start.4 = (bf16[512,256]{1,0:T(8,128)(2,1)S(1)}, bf16[512,256]{1,0:T(8,128)(2,1)}, u32[]{:S(2)}) copy-start(bf16[512,256]{1,0:T(8,128)(2,1)} %param.28) | copy-start | bytes 786436
  37.6 568.1 %copy-start.11 = (f32[256]{0:T(256)S(1)}, f32[256]{0:T(256)}, u32[]{:S(2)}) copy-start(f32[256]{0:T(256)} %param.32) | copy-start | bytes 3076
  690.3 17.3 %copy-start.1 = (f32[8,64,4,128]{3,1,0,2:T(8,128)S(1)}, f32[8,64,4,128]{3,1,0,2:T(8,128)}, u32[]{:S(2)}) copy-start(f32[8,64,4,128]{3,1,0,2:T(8,128)} %get-tuple-element.144) | copy-start | bytes 3145732
  690.4 66.9 %reduce-scatter.3.cloned.1.call-start = ((), (), s32[]{:S(2)}) async-start(), calls=%async_computation.4 | async-start | bytes 2621440 | tf_op jit(solution)/shard_map/reduce_scatter | solution.py:163
  709.2 2.4 copy-start.2
  709.2 2.4 copy-start.7
  709.2 2.4 copy-start.13
  709.2 2.4 copy-start.14
  709.3 2.6 copy-start.6
  709.5 18.9 %copy-start.15 = (bf16[2048,4]{0,1:T(4,128)(2,1)S(1)}, bf16[2048,4]{0,1:T(4,128)(2,1)}, u32[]{:S(2)}) copy-start(bf16[2048,4]{0,1:T(4,128)(2,1)} %param.36) | copy-start | bytes 49156
  722.9 19.8 %all-to-all-start.1 = ((bf16[512,8,1,64]{0,3,2,1:T(8,128)(2,1)}), bf16[512,8,1,64]{0,3,2,1:T(8,128)(2,1)S(1)}, u32[]{:S(2)}, u32[]{:S(2)}) async-start(bf16[512,8,1,64]{0,3,2,1:T(8,128)(2,1)} %bitcast.285), calls=%async_computation.3 | async-start | bytes 1048576 | tf_op jit(solution)/shard_map/all_to_all | solution.py:250
Sparse Core Ops, SparseCore 0:
  37.5 23.9 all-gather.3
  690.5 32.3 reduce-scatter.4
  726.0 31.1 reduce-scatter.2
where the time goes:
time: 769 us; the launch traced here: 764 us
  other arithmetic  347 us (45%)
  local copies, waits for them, and re-layouts  220 us (29%)
  blocking collectives  67.4 us (9%)
  matrix products  61.2 us (8%)
  waiting for transfers between devices  38.2 us (5%)
  between operations  14.2 us (2%)
  starting transfers between devices  13.5 us (2%)
    while x24, local copies, waits for them, and re-layouts  171 us
    while x16, other arithmetic  162 us
    another operation x40, other arithmetic, block_advance(): jax.scipy.linalg.solve_triangular(left_side, right_side, lower=True, unit...  158 us
    all_gather x2, blocking collectives, carried_in(): lax.all_gather(part.astype(kind), axis)  67.4 us
    squeeze x48, local copies, waits for them, and re-layouts, mixer_part(): lax.scan(block_advance, start, (blocked(recept), blocked(decay_logarithm)...  19 us
  transfers between devices with their start and end apart: 5, of which 3 were waited for; matrix products, arithmetic and copies ran while one was open for 79% of the time, Pallas kernels for 0%

commit v1 on v0

v1 whole, which is shorter than its diff:
```python
import functools
import math

import jax
import jax.numpy as jnp
from jax import lax
from jax.experimental import pallas as pl
from jax.experimental.pallas import tpu as pltpu
from jax.sharding import PartitionSpec as P

HEAD_DIM = 64
PAIR = 2 * HEAD_DIM
HALF_EXP = math.exp(-0.5)
GROUPS = 4


key_eps = 1e-06
group_eps = 0.00064
norm_eps = 1e-06
highest = lax.Precision.HIGHEST


def bf(x):
    return x.astype(jnp.bfloat16)


def mm(x, y):
    return lax.dot_general(x, y, (((1,), (0,)), ((), ())), preferred_element_type=jnp.float32)


def mm_nt(x, y):
    return lax.dot_general(x, y, (((1,), (1,)), ((), ())), preferred_element_type=jnp.float32)


def mm_tn(x, y):
    return lax.dot_general(x, y, (((0,), (0,)), ((), ())), preferred_element_type=jnp.float32)


def halves(x):
    high = bf(x)
    return high, bf(x - high.astype(jnp.float32))


def sum_right(x, ones):
    high, low = halves(x)
    return mm(high, ones) + mm(low, ones)


def logistic(x):
    return 1.0 / (1.0 + jnp.exp(-x))


def flag(cond):
    return jnp.where(cond, 1.0, 0.0)


def iota(shape, dim):
    return lax.broadcasted_iota(jnp.int32, shape, dim)


def pair_blocks():
    return flag((iota((PAIR, PAIR), 0) < HEAD_DIM) == (iota((PAIR, PAIR), 1) < HEAD_DIM))


def scan_kernel(
    group,
    r_ref,
    k_ref,
    v_ref,
    d_ref,
    a_ref,
    d_off_ref,
    a_off_ref,
    extra_ref,
    out_ref,
    reach_ref,
    ends_ref,
    chain_ref,
):
    positions, width = r_ref.shape
    pairs = width // PAIR
    C = HEAD_DIM
    rows_per = group * C
    own_block = pair_blocks()
    own_bf = bf(own_block)
    row, col = iota((C, PAIR), 0), iota((C, PAIR), 1) & (HEAD_DIM - 1)
    strict, upto = row > col, row >= col
    eye = flag(row == col)
    first = iota((1, PAIR), 1) < HEAD_DIM
    tri = bf(flag(iota((C, C), 0) >= iota((C, C), 1)))
    level_masks = []
    for s in range(6):
        inside = (
            ((row >> (s + 1)) == (col >> (s + 1)))
            & (((row >> s) & 1) == 1)
            & (((col >> s) & 1) == 0)
        )
        level_masks.append(bf(flag(inside)))

    def spread(x):
        return jnp.concatenate([x, x], axis=0) * own_bf

    square = (iota((PAIR, PAIR), 0) == iota((PAIR, PAIR), 1)).astype(jnp.float32)
    for p in range(pairs):
        chain_ref[p, :PAIR] = jnp.zeros((PAIR, PAIR), jnp.float32)
        chain_ref[p, PAIR:] = square

    def step(g, carry):
        base = pl.multiple_of(g * rows_per, rows_per)
        rows = pl.ds(base, rows_per)
        items = []
        for p in range(pairs):
            lanes = slice(p * PAIR, (p + 1) * PAIR)
            k = k_ref[rows, lanes].astype(jnp.float32)
            u = k * lax.rsqrt(sum_right(k * k, own_bf) + key_eps)
            rem = u * logistic(a_ref[rows, lanes].astype(jnp.float32) + a_off_ref[:, lanes])
            e = extra_ref[rows, :]
            extra = jnp.where(first, e[:, 2 * p : 2 * p + 1], e[:, 2 * p + 1 : 2 * p + 2])
            lg = extra - HALF_EXP * logistic(
                d_ref[rows, lanes].astype(jnp.float32) + d_off_ref[:, lanes]
            )
            r = r_ref[rows, lanes].astype(jnp.float32)
            v = v_ref[rows, lanes]
            for c in range(group):
                cut = slice(c * C, (c + 1) * C)
                items.append((p, c, k[cut], u[cut], rem[cut], lg[cut], r[cut], v[cut]))
        stage = []
        for p, c, k, u, rem, lg, r, v in items:
            high, low = halves(lg)
            rest = bf(lg - high.astype(jnp.float32) - low.astype(jnp.float32))
            cumul = mm(tri, high) + mm(tri, low) + mm(tri, rest)
            stage.append(cumul)
        work = []
        for (p, c, k, u, rem, lg, r, v), cumul in zip(items, stage):
            mid = 0.5 * cumul[C - 1 : C]
            up_now, down = jnp.exp(cumul - mid), jnp.exp(mid - cumul)
            up_before = jnp.exp(cumul - lg - mid)
            half = jnp.exp(mid)
            cq, cu, dk, dr = r * up_now, u * up_before, k * down, rem * down
            left = bf(jnp.concatenate([cu, cq], axis=0))
            pair_r = mm_nt(left, spread(bf(dr)))
            pair_k = mm_nt(left, spread(bf(dk)))
            work.append((cq * half, bf(cu * half), bf(dk * half), bf(dr * half), half * half, pair_r, pair_k))
        solve = []
        for (p, c, k, u, rem, lg, r, v), (qe, ue, kt, rt, ed, pair_r, pair_k) in zip(items, work):
            rp = bf(jnp.where(strict, pair_r[:C], 0.0))
            rr = bf(jnp.where(upto, pair_r[C:], 0.0))
            kp = jnp.where(strict, pair_k[:C], 0.0)
            rk = jnp.where(upto, pair_k[C:], 0.0)
            kv = mm(bf(jnp.concatenate([kp, rk], axis=0)), spread(v))
            inv = eye - (rp * level_masks[0]).astype(jnp.float32)
            solve.append([rp, rr, kv, inv])
        for s in range(1, 6):
            mids = [bf(mm(bf(inv), spread(rp * level_masks[s]))) for rp, rr, kv, inv in solve]
            for item, y in zip(solve, mids):
                item[3] = item[3] - mm(y, spread(bf(item[3])))
        wvs = []
        for (rp, rr, kv, inv), w in zip(solve, work):
            wide = jnp.concatenate([spread(w[1]), spread(bf(kv[:C]))], axis=1)
            wvs.append(bf(mm(bf(inv), wide)))
        tails = []
        for (rp, rr, kv, inv), (qe, ue, kt, rt, ed, _, _), wv, item in zip(solve, work, wvs, items):
            wide = jnp.concatenate([spread(wv[:, :PAIR]), spread(wv[:, PAIR:])], axis=1)
            rw = mm(rr, wide)
            read = bf(qe - rw[:, :PAIR])
            local = kv[C:] - rw[:, PAIR:]
            v = item[7]
            x = jnp.concatenate(
                [jnp.concatenate([v, jnp.zeros_like(v)], axis=1),
                 jnp.concatenate([-wv[:, PAIR:], -wv[:, :PAIR]], axis=1)], axis=0)
            nb = mm_tn(x, jnp.concatenate([kt, rt], axis=0))
            tails.append((read, local, nb[:PAIR] * own_block, bf(nb[PAIR:] * own_block), ed))
        z = [chain_ref[p] for p in range(pairs)]
        for c in range(group):
            for p in range(pairs):
                read, local, add, neg, ed = tails[p * group + c]
                zb = bf(z[p])
                qz = mm_nt(read, zb)
                at = pl.ds(pl.multiple_of(base + c * C, C), C)
                lanes = slice(p * PAIR, (p + 1) * PAIR)
                out_ref[at, lanes] = local + qz[:, :PAIR]
                reach_ref[at, lanes] = bf(qz[:, PAIR:])
                moved = z[p] * ed + mm(zb, neg)
                z[p] = jnp.concatenate([moved[:PAIR] + add, moved[PAIR:]], axis=0)
        for p in range(pairs):
            chain_ref[p] = z[p]
        return carry

    lax.fori_loop(0, positions // rows_per, step, 0)
    for p in range(pairs):
        s, m = chain_ref[p, :PAIR], chain_ref[p, PAIR:]
        ends_ref[p * 2 * C : p * 2 * C + C] = bf(s[:C] + s[C:])
        ends_ref[p * 2 * C + C : (p + 1) * 2 * C] = bf(m[:C] + m[C:])


def join_kernel(axis, all_ref, out_ref, reach_ref, gate_ref, gain_ref, mixed_ref):
    devices, place = lax.axis_size(axis), lax.axis_index(axis)
    width = out_ref.shape[1]
    pairs = width // PAIR
    C = HEAD_DIM
    own_block = pair_blocks()
    own_bf = bf(own_block)
    mean_bf = bf(own_block * (1.0 / HEAD_DIM))
    states = [jnp.zeros((C, PAIR), jnp.float32) for _ in range(pairs)]

    def hop(j, states):
        new = []
        for p in range(pairs):
            s = all_ref[j, p * 2 * C : p * 2 * C + C].astype(jnp.float32)
            m = all_ref[j, p * 2 * C + C : (p + 1) * 2 * C]
            m = jnp.concatenate([m, m], axis=0) * own_bf
            new.append(sum_right(states[p], m) + s)
        return tuple(new)

    states = lax.fori_loop(0, place, hop, tuple(states))
    for p in range(pairs):
        lanes = slice(p * PAIR, (p + 1) * PAIR)
        s = bf(states[p])
        s = jnp.concatenate([s, s], axis=0) * own_bf
        head = out_ref[:, lanes] + mm_nt(reach_ref[:, lanes], s)
        centred = head - sum_right(head, mean_bf)
        spread = sum_right(centred * centred, mean_bf)
        normed = centred * lax.rsqrt(spread + group_eps)
        gate = logistic(gate_ref[:, lanes].astype(jnp.float32))
        mixed_ref[:, lanes] = bf(normed * gain_ref[:, lanes] * gate)


def mixer_part(
    receptance,
    key_matrix,
    value_matrix,
    decay_data_term,
    correction_rate_data,
    output_gate_input,
    decay_channel_offset,
    correction_rate_offset,
    extra_head_log_decay,
    head_norm_gain,
    mixer_output_weight,
):
    positions, own_width = receptance.shape
    pairs = -(-own_width // PAIR)
    width = pairs * PAIR

    def filled(x, columns=width):
        return x if x.shape[-1] == columns else jnp.pad(x, ((0, 0), (0, columns - x.shape[-1])))

    whole_weight = lax.all_gather(mixer_output_weight, "tp", axis=0, tiled=True)
    blocks = positions // HEAD_DIM
    group = 4 if blocks % 4 == 0 else 1
    local, reach, ends = pl.pallas_call(
        functools.partial(scan_kernel, group),
        out_shape=(
            jax.ShapeDtypeStruct((positions, width), jnp.float32),
            jax.ShapeDtypeStruct((positions, width), jnp.bfloat16),
            jax.ShapeDtypeStruct((pairs * 2 * HEAD_DIM, PAIR), jnp.bfloat16),
        ),
        scratch_shapes=[pltpu.VMEM((pairs, 2 * PAIR, PAIR), jnp.float32)],
        cost_estimate=pl.CostEstimate(
            flops=60000 * positions * width, bytes_accessed=16 * positions * width, transcendentals=0
        ),
    )(
        filled(receptance),
        filled(key_matrix),
        filled(value_matrix),
        filled(decay_data_term),
        filled(correction_rate_data),
        filled(decay_channel_offset[None]),
        filled(correction_rate_offset[None]),
        filled(extra_head_log_decay, 2 * pairs),
    )
    everyone = lax.all_gather(ends, "ep")
    mixed_hidden = pl.pallas_call(
        functools.partial(join_kernel, "ep"),
        out_shape=jax.ShapeDtypeStruct((positions, width), jnp.bfloat16),
        cost_estimate=pl.CostEstimate(
            flops=6000 * positions * width, bytes_accessed=16 * positions * width, transcendentals=0
        ),
    )(everyone, local, reach, filled(output_gate_input), filled(head_norm_gain[None]))
    mixed_hidden = mixed_hidden[:, :own_width]
    own_rows = lax.all_to_all(mixed_hidden, "tp", split_axis=0, concat_axis=1, tiled=True)
    return jnp.dot(own_rows, whole_weight, preferred_element_type=jnp.float32).astype(jnp.bfloat16)


def finish_experts(gate_val, up_val, expert_down_weight):
    expert_hidden = (jax.nn.silu(gate_val) * up_val).astype(jnp.bfloat16)
    return lax.psum_scatter(
        jnp.einsum(
            "sxcf,xfd->dsxc", expert_hidden, expert_down_weight, preferred_element_type=jnp.float32
        ).astype(jnp.bfloat16),
        "tp",
        scatter_dimension=0,
        tiled=True,
    )


def expert_part(
    expert_layer_input,
    feedforward_norm_gain,
    group_router_weight,
    expert_router_weight,
    routes,
    expert_gate_weight,
    expert_up_weight,
    expert_down_weight,
):
    token_rows = expert_layer_input.shape[0]
    route_count = routes.shape[1]
    ep_count = lax.axis_size("ep")
    expert_total = expert_router_weight.shape[1]
    per_group = expert_total // GROUPS
    capacity = 4 * token_rows // ep_count
    widened = expert_layer_input.astype(jnp.float32)
    normed_input = (
        widened
        * lax.rsqrt(jnp.mean(widened * widened, axis=-1, keepdims=True) + norm_eps)
        * feedforward_norm_gain
    ).astype(jnp.bfloat16)
    group_logit = jnp.dot(normed_input, group_router_weight, preferred_element_type=jnp.float32)
    group_exp = jnp.exp(group_logit)
    group_prob = group_exp / jnp.sum(group_exp, axis=-1, keepdims=True)
    expert_logit = jnp.dot(normed_input, expert_router_weight, preferred_element_type=jnp.float32)
    expert_range = jnp.arange(expert_total, dtype=jnp.int32)
    matched = routes[:, :, None] == expert_range[None, None, :]
    chosen_logit = jnp.sum(jnp.where(matched, expert_logit[:, None, :], 0.0), axis=-1)
    group_match = (routes // per_group)[:, :, None] == jnp.arange(GROUPS, dtype=jnp.int32)[
        None, None, :
    ]
    chosen_group = jnp.sum(jnp.where(group_match, group_prob[:, None, :], 0.0), axis=-1)
    route_weight = chosen_group * jax.nn.sigmoid(chosen_logit - chosen_logit[:, ::-1])
    flat_match = matched.reshape(token_rows * route_count, expert_total).astype(jnp.int32)
    before = jnp.cumsum(flat_match, axis=0) - flat_match
    placed = jnp.sum(before * flat_match, axis=1)
    slot_ids = routes.reshape(-1) * capacity + placed
    slot_range = jnp.arange(expert_total * capacity, dtype=jnp.int32)
    struck = (slot_range[:, None] == slot_ids[None, :]).reshape(
        expert_total * capacity, token_rows, route_count
    )
    dispatch_matrix = jnp.any(struck, axis=-1).astype(jnp.bfloat16)
    combine_matrix = jnp.sum(jnp.where(struck, route_weight[None, :, :], 0.0), axis=-1)
    outgoing = jnp.dot(dispatch_matrix, normed_input, preferred_element_type=jnp.float32).astype(
        jnp.bfloat16
    )
    outgoing = outgoing.reshape(ep_count, expert_total // ep_count, capacity, outgoing.shape[1])
    width_share = outgoing.shape[3] // lax.axis_size("tp")
    own_columns = lax.dynamic_slice_in_dim(
        outgoing, lax.axis_index("tp") * width_share, width_share, 3
    )
    piece = lax.all_gather(
        lax.all_to_all(own_columns, "ep", split_axis=0, concat_axis=0, tiled=True),
        "tp",
        axis=3,
        tiled=True,
    )
    gate_val = jnp.einsum(
        "sxcd,xdf->sxcf", piece, expert_gate_weight, preferred_element_type=jnp.float32
    )
    up_val = jnp.einsum(
        "sxcd,xdf->sxcf", piece, expert_up_weight, preferred_element_type=jnp.float32
    )
    expert_rows = finish_experts(gate_val, up_val, expert_down_weight)
    homebound = lax.all_to_all(expert_rows, "ep", split_axis=1, concat_axis=1, tiled=True)
    homebound = homebound.reshape(homebound.shape[0], expert_total * capacity)
    combined = jnp.dot(homebound.astype(jnp.float32), combine_matrix, precision=highest)
    return combined.T.astype(jnp.bfloat16)


def local(
    receptance,
    key_matrix,
    value_matrix,
    decay_data_term,
    correction_rate_data,
    output_gate_input,
    decay_channel_offset,
    correction_rate_offset,
    extra_head_log_decay,
    head_norm_gain,
    mixer_output_weight,
    expert_layer_input,
    feedforward_norm_gain,
    group_router_weight,
    expert_router_weight,
    routes,
    expert_gate_weight,
    expert_up_weight,
    expert_down_weight,
):
    token_mixer_output = mixer_part(
        receptance,
        key_matrix,
        value_matrix,
        decay_data_term,
        correction_rate_data,
        output_gate_input,
        decay_channel_offset,
        correction_rate_offset,
        extra_head_log_decay,
        head_norm_gain,
        mixer_output_weight,
    )
    expert_out = expert_part(
        expert_layer_input,
        feedforward_norm_gain,
        group_router_weight,
        expert_router_weight,
        routes,
        expert_gate_weight,
        expert_up_weight,
        expert_down_weight,
    )
    return (token_mixer_output, expert_out)


def solution(mesh):
    in_specs = (
        P("ep", "tp"),
        P("ep", "tp"),
        P("ep", "tp"),
        P("ep", "tp"),
        P("ep", "tp"),
        P("ep", "tp"),
        P("tp"),
        P("tp"),
        P("ep", "tp"),
        P("tp"),
        P("tp", None),
        P("ep", None),
        P(),
        P(),
        P(),
        P("ep", None),
        P("ep", None, "tp"),
        P("ep", None, "tp"),
        P("ep", "tp", None),
    )
    out_specs = (P(("ep", "tp"), None), P("ep", "tp"))
    return jax.shard_map(local, mesh=mesh, in_specs=in_specs, out_specs=out_specs, check_vma=False)
```

time: 769 us -> 164 us (0.21)
  other arithmetic: 347 us -> 2.85 us
  local copies, waits for them, and re-layouts: 220 us -> 4.26 us
  matrix products: 61.2 us -> 24 us
  blocking collectives: 67.4 us -> 55.2 us
  Pallas kernels: 0 us -> 11.4 us
    while x26 -> x0, local copies, waits for them, and re-layouts: 172 us -> none
    another operation x50 -> x2, other arithmetic: 167 us -> 0.62 us  [the longest x40 158 us: block_advance(): jax.scipy.linalg.solve_triangular(left_side, right_side, lower=True, unit...]
    while x16 -> x0, other arithmetic: 162 us -> none
    all_gather x2 -> x1, blocking collectives: 67.4 us -> 33.5 us  [mixer_part(): everyone = lax.all_gather(ends, 'ep')]
    dot_general x66 -> x1, matrix products: 37.4 us -> 3.73 us  [mixer_part(): jnp.dot(own_rows, whole_weight, preferred_element_type=jnp.float32)]
    all_gather x1, waiting for transfers between devices: 0.01 us -> 21.7 us  [expert_part(): lax.all_gather(lax.all_to_all(own_columns, 'ep', split_axis=0, concat_axi...]
    all_to_all x0 -> x1, blocking collectives: none -> 21.7 us  [expert_part(): lax.all_to_all(own_columns, 'ep', split_axis=0, concat_axis=0, tiled=True)]
    squeeze x56 -> x0, local copies, waits for them, and re-layouts: 19 us -> none  [the longest x48 19 us: mixer_part(): lax.scan(block_advance, start, (blocked(recept), blocked(decay_logarithm)...]
  transfers between devices with their start and end apart: 5 -> 5, of which waited for: 3 -> 4; matrix products, arithmetic and copies ran while one was open for 79% -> 4% of each run, Pallas kernels for 0% -> 7%
where the time goes in v1:
time: 164 us; the launch traced here: 163 us
  blocking collectives  55.2 us (34%)
  waiting for transfers between devices  41.5 us (25%)
  matrix products  24 us (15%)
  between operations  13.9 us (8%)
  Pallas kernels  11.4 us (7%)
  starting transfers between devices  10.4 us (6%)
  local copies, waits for them, and re-layouts  4.26 us (3%)
  other arithmetic  2.85 us (2%)
    all_gather x1, blocking collectives, mixer_part(): everyone = lax.all_gather(ends, 'ep')  33.5 us
    all_gather x1, waiting for transfers between devices, expert_part(): lax.all_gather(lax.all_to_all(own_columns, 'ep', split_axis=0, concat_axi...  21.7 us
    all_to_all x1, blocking collectives, expert_part(): lax.all_to_all(own_columns, 'ep', split_axis=0, concat_axis=0, tiled=True)  21.7 us
    dot_general x1, matrix products, finish_experts(): jnp.einsum('sxcf,xfd->dsxc', expert_hidden, expert_down_weight, preferred...  10.1 us
    all_to_all x1, waiting for transfers between devices, mixer_part(): lax.all_to_all(mixed_hidden, 'tp', split_axis=0, concat_axis=1, tiled=True)  8.51 us
    pallas_call x1, Pallas kernels, mixer_part(): pl.pallas_call(functools.partial(scan_kernel, group), out_shape=(jax.Shap...  8.46 us
    all_to_all x1, waiting for transfers between devices, expert_part(): lax.all_to_all(expert_rows, 'ep', split_axis=1, concat_axis=1, tiled=True)  8.33 us
    all_to_all x1, starting transfers between devices, expert_part(): lax.all_to_all(expert_rows, 'ep', split_axis=1, concat_axis=1, tiled=True)  6.88 us
  transfers between devices with their start and end apart: 5, of which 4 were waited for; matrix products, arithmetic and copies ran while one was open for 4% of the time, Pallas kernels for 7%

profile of v1, /device:TPU:0, one launch (start us, length us, event | category | flops | bytes accessed | tf_op | source)
XLA Modules:
  0.0 163.5 jit_solution(13679173505643668884)
XLA Ops:
  7.2 0.0 copy-start
  7.2 0.0 all-gather.6.cloned.1.call-start
  7.2 0.8 copy.62
  8.0 0.1 eq.64
  8.2 0.1 eq.60
  8.3 0.6 reduce-window.6
  8.9 0.2 slice_reduce_fusion
  9.2 0.1 fusion.36
  9.2 0.1 reduce_sum.57
  9.4 0.1 copy.64
  9.5 0.7 multiply_add_fusion
  10.2 0.1 fusion.34
  10.2 1.2 fusion.27
  11.5 1.8 %convolution_convert_fusion = bf16[512,2048]{1,0:T(8,128)(2,1)S(1)} fusion(pred[512,128]{1,0:T(8,128)(4,1)S(1)} %fusion.34, bf16[128,2048]{1,0:T(8,128)(2,1)} %param.30, f32[2048]{0:T(1024)} %param.31, f32[128]{0:T(128)S(1)} %add_rsqrt_fusion), kind=kOutput, calls=%fused_computation.7 | convolution fusion | flops 270532608 | bytes 2695680 | tf_op jit(solution)/shard_map/dot_general | solution.py:341
  13.4 21.7 %all_to_all.29 = bf16[8,1,64,512]{3,2,1,0:T(8,128)(2,1)} all-to-all(bf16[8,1,64,512]{3,2,1,0:T(8,128)(2,1)S(1)} %constant_dynamic-slice_fusion), channel_id=1, replica_groups=mesh['ep'=8,'tp'=4] {'ep'}, dimensions={0} | all-to-all | bytes 1048576 | tf_op jit(solution)/shard_map/all_to_all | solution.py:350
  35.1 0.0 all-gather.6.cloned.1.call-update
  35.1 0.0 reduce-scatter.2.cloned.1.call-start
  35.1 21.7 %all-gather.6.cloned.1.call-done = bf16[8,1,64,2048]{3,2,0,1:T(8,128)(2,1)} async-done(((bf16[8,1,64,512]{3,2,0,1:T(8,128)(2,1)}), bf16[8,1,64,2048]{3,2,0,1:T(8,128)(2,1)}) %all-gather.6.cloned.1.call-update) | async-done | bytes 2097168 | tf_op jit(solution)/shard_map/all_gather | solution.py:349
  56.9 0.0 copy-start.5
  56.9 6.6 %fusion.2 = f32[8,64,1024]{2,1,0:T(8,128)} fusion(bf16[1,2048,1024]{2,1,0:T(8,128)(2,1)} %param.36, bf16[8,1,64,2048]{3,2,0,1:T(8,128)(2,1)} %all-gather.6.cloned.1.call-done), kind=kOutput, calls=%fused_computation.2 | convolution fusion | flops 2147483648 | bytes 8388608 | tf_op jit(solution)/shard_map/sxcd,xdf->sxcf/dot_general | solution.py:358
  63.4 0.0 copy-done.5
  63.4 10.1 %fusion.9 = bf16[2048,8,1,64]{0,3,1,2:T(8,128)(2,1)} fusion(bf16[1,1024,2048]{2,1,0:T(8,128)(2,1)} %param.37, f32[8,64,1024]{2,1,0:T(8,128)} %fusion.2, bf16[1,2048,1024]{2,1,0:T(8,128)(2,1)} %param.35, bf16[8,1,64,2048]{3,2,0,1:T(8,128)(2,1)S(1)} %copy-done.5), kind=kOutput, calls=%fused_computation.8 | convolution fusion | flops 4299161600 | bytes 14680064 | tf_op jit(solution)/shard_map/sxcf,xfd->dsxc/dot_general | solution.py:288
  73.6 0.0 copy-start.4
  73.6 0.0 reduce-scatter.2.cloned.1.call-update
  73.6 0.0 all-gather.4.cloned.1.call-start
  73.6 0.7 all-gather.4.cloned.1.call-update
  74.3 0.0 copy-done.4
  74.3 0.9 copy.60.extra_ref
  75.2 8.5 %shard_map.194 = (f32[512,256]{1,0:T(8,128)}, bf16[512,256]{1,0:T(8,128)(2,1)}, bf16[256,128]{1,0:T(8,128)(2,1)}) custom-call(bf16[512,256]{1,0:T(8,128)(2,1)} %r_ref.1, bf16[512,256]{1,0:T(8,128)(2,1)} %k_ref.1, bf16[512,256]{1,0:T(8,128)(2,1)} %v_ref.1, bf16[512,256]{1,0:T(8,128)(2,1)} %d_ref.1, bf16[512,256]{1,0:T(8,128)(2,1)} %a_ref.1, ...), custom_call_target="tpu_custom_call" | custom-call | flops 7864320000 | bytes 2097152 | tf_op jit(solution)/shard_map/pallas_call | solution.py:251
  83.7 33.5 %all-gather = bf16[2048,128]{1,0:T(8,128)(2,1)} all-gather(bf16[256,128]{1,0:T(8,128)(2,1)} %get-tuple-element.5), channel_id=2, replica_groups=mesh['ep'=8,'tp'=4] {'ep'}, dimensions={0}, use_global_device_ids=true | all-gather | bytes 589824 | tf_op jit(solution)/shard_map/all_gather | solution.py:272
  117.2 0.0 copy-start.1
  117.2 3.0 %shard_map.195 = bf16[512,256]{1,0:T(8,128)(2,1)} custom-call(bf16[8,256,128]{2,1,0:T(8,128)(2,1)} %bitcast.107, f32[512,256]{1,0:T(8,128)} %get-tuple-element.6.out_ref, bf16[512,256]{1,0:T(8,128)(2,1)} %get-tuple-element.7.reach_ref, bf16[512,256]{1,0:T(8,128)(2,1)} %gate_ref.1, f32[1,256]{1,0:T(1,128)} %bitcast.112), custom_call_target="tpu_custom_call" | custom-call | flops 786432000 | bytes 2097152 | tf_op jit(solution)/shard_map/pallas_call | solution.py:273
  120.2 1.8 %copy.61 = bf16[4,128,256]{1,2,0:T(8,128)(2,1)} copy(bf16[4,128,256]{2,1,0:T(8,128)(2,1)} %bitcast.109) | data formatting | bytes 524288 | tf_op jit(solution)/shard_map/all_to_all | solution.py:281
  122.0 3.4 %all-to-all-start = ((bf16[4,128,256]{1,2,0:T(8,128)(2,1)}), bf16[4,128,256]{1,2,0:T(8,128)(2,1)S(1)}, u32[]{:S(2)}, u32[]{:S(2)}) async-start(bf16[4,128,256]{1,2,0:T(8,128)(2,1)} %copy.61), calls=%async_computation | async-start | bytes 524288 | tf_op jit(solution)/shard_map/all_to_all | solution.py:281
  125.4 0.0 copy-done.1
  125.4 0.0 copy-done.3
  125.4 0.0 copy-done.6
  125.4 0.3 fusion.43
  125.7 0.0 copy-done
  125.7 0.3 fusion.40
  126.1 8.5 %all-to-all-done = bf16[4,128,256]{1,2,0:T(8,128)(2,1)S(1)} async-done(((bf16[4,128,256]{1,2,0:T(8,128)(2,1)}), bf16[4,128,256]{1,2,0:T(8,128)(2,1)S(1)}, u32[]{:S(2)}, u32[]{:S(2)}) %all-to-all-start) | async-done | bytes 262176 | tf_op jit(solution)/shard_map/all_to_all | solution.py:281
  134.6 6.9 %all-to-all-start.2 = ((bf16[512,8,1,64]{0,3,2,1:T(8,128)(2,1)}), bf16[512,8,1,64]{0,3,2,1:T(8,128)(2,1)S(1)}, u32[]{:S(2)}, u32[]{:S(2)}) async-start(bf16[512,8,1,64]{0,3,2,1:T(8,128)(2,1)} %bitcast.108), calls=%async_computation.3 | async-start | bytes 1048576 | tf_op jit(solution)/shard_map/all_to_all | solution.py:362
  141.4 0.0 copy-done.2
  141.5 0.1 select_reduce_fusion
  141.6 2.2 %all-gather.4.cloned.1.call-done = bf16[1024,2048]{1,0:T(8,128)(2,1)} async-done(((bf16[256,2048]{1,0:T(8,128)(2,1)}), bf16[1024,2048]{1,0:T(8,128)(2,1)}) %all-gather.4.cloned.1.call-update) | async-done | bytes 4194320 | tf_op jit(solution)/shard_map/all_gather | solution.py:248
  143.8 3.7 %convolution_convert_fusion.1 = bf16[128,2048]{1,0:T(8,128)(2,1)} fusion(bf16[128,1024]{0,1:T(8,128)(2,1)S(1)} %bitcast.106, bf16[1024,2048]{1,0:T(8,128)(2,1)} %all-gather.4.cloned.1.call-done), kind=kOutput, calls=%fused_computation.9 | convolution fusion | flops 537133056 | bytes 4980736 | tf_op jit(solution)/shard_map/dot_general | solution.py:282
  147.5 8.3 %all-to-all-done.2 = bf16[512,8,1,64]{0,3,2,1:T(8,128)(2,1)S(1)} async-done(((bf16[512,8,1,64]{0,3,2,1:T(8,128)(2,1)}), bf16[512,8,1,64]{0,3,2,1:T(8,128)(2,1)S(1)}, u32[]{:S(2)}, u32[]{:S(2)}) %all-to-all-start.2) | async-done | bytes 524320 | tf_op jit(solution)/shard_map/all_to_all | solution.py:362
  155.9 1.1 convolution_convert_fusion.2
  (14 shorter events, 0.2 us)
Async XLA Ops:
  7.2 118.6 %copy-start = (bf16[2048,8]{0,1:T(8,128)(2,1)S(1)}, bf16[2048,8]{0,1:T(8,128)(2,1)}, u32[]{:S(2)}) copy-start(bf16[2048,8]{0,1:T(8,128)(2,1)} %param.33) | copy-start | bytes 98308
  7.2 49.7 %all-gather.6.cloned.1.call-start = ((), (), s32[]{:S(2)}) async-start(), calls=%async_computation.5 | async-start | bytes 2621440 | tf_op jit(solution)/shard_map/all_gather | solution.py:349
  35.1 99.5 %reduce-scatter.2.cloned.1.call-start = ((), (), s32[]{:S(2)}) async-start(), calls=%async_computation.6 | async-start | bytes 2621440 | tf_op jit(solution)/shard_map/reduce_scatter | solution.py:287
  56.9 6.6 %copy-start.5 = (bf16[8,1,64,2048]{3,2,0,1:T(8,128)(2,1)S(1)}, bf16[8,1,64,2048]{3,2,0,1:T(8,128)(2,1)}, u32[]{:S(2)}) copy-start(bf16[8,1,64,2048]{3,2,0,1:T(8,128)(2,1)} %all-gather.6.cloned.1.call-done) | copy-start | bytes 6291460
  73.6 0.8 copy-start.4
  73.6 70.2 %all-gather.4.cloned.1.call-start = ((), (), s32[]{:S(2)}) async-start(), calls=%async_computation.4 | async-start | bytes 5242880 | tf_op jit(solution)/shard_map/all_gather | solution.py:248
  117.2 8.2 %copy-start.1 = (bf16[128,2048]{1,0:T(8,128)(2,1)S(1)}, bf16[128,2048]{1,0:T(8,128)(2,1)}, u32[]{:S(2)}) copy-start(bf16[128,2048]{1,0:T(8,128)(2,1)} %param.30) | copy-start | bytes 1572868
  117.2 8.2 %copy-start.3 = (f32[2048]{0:T(1024)S(1)}, f32[2048]{0:T(1024)}, u32[]{:S(2)}) copy-start(f32[2048]{0:T(1024)} %param.31) | copy-start | bytes 24580
  117.2 8.2 %copy-start.6 = (bf16[2048,4]{0,1:T(4,128)(2,1)S(1)}, bf16[2048,4]{0,1:T(4,128)(2,1)}, u32[]{:S(2)}) copy-start(bf16[2048,4]{0,1:T(4,128)(2,1)} %param.32) | copy-start | bytes 49156
  120.1 21.3 %copy-start.2 = (s32[128,2]{0,1:T(2,128)S(1)}, s32[128,2]{0,1:T(2,128)}, u32[]{:S(2)}) copy-start(s32[128,2]{0,1:T(2,128)} %param.34) | copy-start | bytes 3076
  122.0 12.6 %all-to-all-start = ((bf16[4,128,256]{1,2,0:T(8,128)(2,1)}), bf16[4,128,256]{1,2,0:T(8,128)(2,1)S(1)}, u32[]{:S(2)}, u32[]{:S(2)}) async-start(bf16[4,128,256]{1,2,0:T(8,128)(2,1)} %copy.61), calls=%async_computation | async-start | bytes 524288 | tf_op jit(solution)/shard_map/all_to_all | solution.py:281
  134.6 21.3 %all-to-all-start.2 = ((bf16[512,8,1,64]{0,3,2,1:T(8,128)(2,1)}), bf16[512,8,1,64]{0,3,2,1:T(8,128)(2,1)S(1)}, u32[]{:S(2)}, u32[]{:S(2)}) async-start(bf16[512,8,1,64]{0,3,2,1:T(8,128)(2,1)} %bitcast.108), calls=%async_computation.3 | async-start | bytes 1048576 | tf_op jit(solution)/shard_map/all_to_all | solution.py:362
Sparse Core Ops, SparseCore 0:
  35.2 21.5 all-gather.5
  73.7 31.1 reduce-scatter.1
  106.5 37.2 all-gather.3

commit v2 on v1

--- a/solution.py
+++ b/solution.py
@@ -225,7 +225,321 @@
         mixed_ref[:, lanes] = bf(normed * gain_ref[:, lanes] * gate)
 
 
-def mixer_part(
+def place_of():
+    n_ep, n_tp = lax.axis_size("ep"), lax.axis_size("tp")
+    e, t = lax.axis_index("ep"), lax.axis_index("tp")
+    core = lax.rem(t, 2)
+    return n_ep, n_tp, n_tp // 2, e, t, lax.div(t, 2), core
+
+
+def remote(src, dst, send, recv, e, t):
+    return pltpu.make_async_remote_copy(
+        src_ref=src,
+        dst_ref=dst,
+        send_sem=send,
+        recv_sem=recv,
+        device_id=(e, t),
+        device_id_type=pl.DeviceIdType.MESH,
+    )
+
+
+def meet():
+    n_ep, n_tp, n_y, e, t, y, core = place_of()
+    barrier = pltpu.get_barrier_semaphore()
+
+    def greet(pe, pt):
+        pl.semaphore_signal(
+            barrier, inc=1, device_id=(pe, pt), device_id_type=pl.DeviceIdType.MESH
+        )
+
+    for d in range(1, n_ep):
+        greet(lax.rem(e + d, n_ep), t)
+    greet(e, 2 * y + 1 - core)
+    for d in range(1, n_y):
+        greet(e, 2 * lax.rem(y + d, n_y) + core)
+    pl.semaphore_wait(barrier, n_ep - 1 + n_y)
+
+
+def dispatch_kernel(
+    cols_ref, ends_ref, piece_ref, every_ref, own_sem, es, er, gs, gr, cs, cr, ys, yr, fs, fr
+):
+    n_ep, n_tp, n_y, e, t, y, core = place_of()
+    share = cols_ref.shape[2]
+    other = 2 * y + 1 - core
+
+    def columns(index):
+        return pl.ds(pl.multiple_of(index * share, share), share)
+
+    def block(source, index):
+        return piece_ref.at[source, :, columns(index)]
+
+    meet()
+    own = pltpu.make_async_copy(cols_ref.at[e], block(e, t), own_sem.at[0])
+    own_ends = pltpu.make_async_copy(ends_ref, every_ref.at[e], own_sem.at[1])
+    own.start()
+    own_ends.start()
+
+    def ep_copy(d):
+        peer = lax.rem(e + d, n_ep)
+        return remote(cols_ref.at[peer], block(e, t), es.at[d], er.at[d], peer, t)
+
+    def ends_copy(d):
+        peer = lax.rem(e + d, n_ep)
+        return remote(ends_ref, every_ref.at[e], gs.at[d], gr.at[d], peer, t)
+
+    def source(d):
+        return lax.rem(e - d + n_ep, n_ep)
+
+    def core_copy(d):
+        return remote(block(source(d), t), block(source(d), t), cs.at[d], cr.at[d], e, other)
+
+    def y_copy(d, h):
+        peer = 2 * lax.rem(y + h, n_y) + core
+        return remote(block(source(d), t), block(source(d), t), ys.at[h, d], yr.at[h, d], e, peer)
+
+    def forward_copy(d, h):
+        index = 2 * lax.rem(y - h + n_y, n_y) + core
+        return remote(
+            block(source(d), index), block(source(d), index), fs.at[h, d], fr.at[h, d], e, other
+        )
+
+    def every(first, body):
+        def run(d, carry):
+            body(d)
+            return carry
+
+        lax.fori_loop(first, n_ep, run, 0)
+
+    every(1, lambda d: ep_copy(d).start())
+    every(1, lambda d: ends_copy(d).start())
+
+    def share_out(d):
+        core_copy(d).start()
+        for h in range(1, n_y):
+            y_copy(d, h).start()
+
+    own.wait()
+    share_out(0)
+
+    def arrived(d):
+        ep_copy(d).wait_recv()
+        share_out(d)
+
+    every(1, arrived)
+
+    def pass_on(d):
+        for h in range(1, n_y):
+            y_copy(d, h).wait_recv()
+            forward_copy(d, h).start()
+
+    every(0, pass_on)
+
+    def close(d):
+        core_copy(d).wait()
+        for h in range(1, n_y):
+            y_copy(d, h).wait_send()
+            forward_copy(d, h).wait()
+
+    every(0, close)
+
+    def close_far(d):
+        ep_copy(d).wait_send()
+        ends_copy(d).wait()
+
+    every(1, close_far)
+    own_ends.wait()
+
+
+def return_kernel(
+    part_ref,
+    proj_ref,
+    home_ref,
+    mixer_ref,
+    near_ref,
+    stage_ref,
+    far_ref,
+    final_ref,
+    mnear_ref,
+    mstage_ref,
+    mfar_ref,
+    own_sem,
+    ns,
+    nr,
+    ys,
+    yr,
+    es,
+    er,
+    mns,
+    mnr,
+    mys,
+    myr,
+):
+    n_ep, n_tp, n_y, e, t, y, core = place_of()
+    share = part_ref.shape[2] // n_tp
+    rows = proj_ref.shape[0] // n_tp
+    other = 2 * y + 1 - core
+
+    def columns(index):
+        return pl.ds(pl.multiple_of(index * share, share), share)
+
+    def row_block(index):
+        return pl.ds(pl.multiple_of(index * rows, rows), rows)
+
+    def peer_y(h):
+        return lax.rem(y + h, n_y)
+
+    def near_copy(s, h):
+        src = part_ref.at[s, :, columns(2 * peer_y(h) + 1 - core)]
+        return remote(src, near_ref.at[s, h], ns.at[s, h], nr.at[s, h], e, other)
+
+    def y_copy(s, h):
+        return remote(
+            stage_ref.at[s, h], far_ref.at[s, h], ys.at[s, h], yr.at[s, h], e, 2 * peer_y(h) + core
+        )
+
+    def home_of(d):
+        return lax.rem(e + d, n_ep)
+
+    def home_copy(d):
+        peer = home_of(d)
+        return remote(final_ref.at[peer], home_ref.at[e], es.at[d], er.at[d], peer, t)
+
+    def mnear_copy(h):
+        src = proj_ref.at[row_block(2 * peer_y(h) + 1 - core), :]
+        return remote(src, mnear_ref.at[h], mns.at[h], mnr.at[h], e, other)
+
+    def my_copy(h):
+        return remote(
+            mstage_ref.at[h], mfar_ref.at[h], mys.at[h], myr.at[h], e, 2 * peer_y(h) + core
+        )
+
+    def every(first, body):
+        def run(d, carry):
+            body(d)
+            return carry
+
+        lax.fori_loop(first, n_ep, run, 0)
+
+    meet()
+
+    def start_near(d):
+        for h in range(n_y):
+            near_copy(home_of(d), h).start()
+
+    every(1, start_near)
+    start_near(0)
+    for h in range(n_y):
+        mnear_copy(h).start()
+
+    def wide(x):
+        return x.astype(jnp.float32)
+
+    def pair_sum(s, h):
+        return wide(part_ref[s, :, columns(2 * peer_y(h) + core)]) + wide(near_ref[s, h])
+
+    def add_near(s):
+        for h in range(1, n_y):
+            near_copy(s, h).wait_recv()
+            stage_ref[s, h] = bf(pair_sum(s, h))
+            y_copy(s, h).start()
+
+    every(1, lambda d: add_near(home_of(d)))
+    add_near(e)
+
+    def mixer_sum(h):
+        return wide(proj_ref[row_block(2 * peer_y(h) + core), :]) + wide(mnear_ref[h])
+
+    for h in range(1, n_y):
+        mnear_copy(h).wait_recv()
+        mstage_ref[h] = bf(mixer_sum(h))
+        my_copy(h).start()
+
+    def add_far(s):
+        near_copy(s, 0).wait_recv()
+        total = pair_sum(s, 0)
+        for h in range(1, n_y):
+            y_copy(s, h).wait_recv()
+            total = total + wide(far_ref[s, h])
+        return bf(total)
+
+    def go_home(d):
+        s = home_of(d)
+        final_ref[s] = add_far(s)
+        home_copy(d).start()
+
+    every(1, go_home)
+    home_ref[e] = add_far(e)
+
+    mnear_copy(0).wait_recv()
+    total = mixer_sum(0)
+    for h in range(1, n_y):
+        my_copy(h).wait_recv()
+        total = total + wide(mfar_ref[h])
+    mixer_ref[...] = bf(total)
+
+    def close(s):
+        for h in range(n_y):
+            near_copy(s, h).wait_send()
+        for h in range(1, n_y):
+            y_copy(s, h).wait_send()
+
+    every(0, close)
+    for h in range(n_y):
+        mnear_copy(h).wait_send()
+    for h in range(1, n_y):
+        my_copy(h).wait_send()
+    every(1, lambda d: home_copy(d).wait())
+
+
+def exchange_out(own_columns, ends):
+    n_ep, n_tp = lax.axis_size("ep"), lax.axis_size("tp")
+    n_y = n_tp // 2
+    capacity, share = own_columns.shape[1:]
+    one, many = pltpu.SemaphoreType.DMA((n_ep,)), pltpu.SemaphoreType.DMA((n_y, n_ep))
+    return pl.pallas_call(
+        dispatch_kernel,
+        out_shape=(
+            jax.ShapeDtypeStruct((n_ep, capacity, n_tp * share), jnp.bfloat16),
+            jax.ShapeDtypeStruct((n_ep, *ends.shape), jnp.bfloat16),
+        ),
+        in_specs=[pl.BlockSpec(memory_space=pltpu.VMEM)] * 2,
+        out_specs=[pl.BlockSpec(memory_space=pltpu.VMEM)] * 2,
+        scratch_shapes=[pltpu.SemaphoreType.DMA((2,))] + [one] * 6 + [many] * 4,
+        compiler_params=pltpu.CompilerParams(collective_id=0, has_side_effects=True),
+    )(own_columns, ends)
+
+
+def exchange_back(partial_rows, projected):
+    n_ep, n_tp = lax.axis_size("ep"), lax.axis_size("tp")
+    n_y = n_tp // 2
+    capacity, model = partial_rows.shape[1:]
+    share, rows = model // n_tp, projected.shape[0] // n_tp
+    many, few = pltpu.SemaphoreType.DMA((n_ep, n_y)), pltpu.SemaphoreType.DMA((n_y,))
+    one = pltpu.SemaphoreType.DMA((n_ep,))
+
+    def held(*shape):
+        return pltpu.VMEM(shape, jnp.bfloat16)
+
+    return pl.pallas_call(
+        return_kernel,
+        out_shape=(
+            jax.ShapeDtypeStruct((n_ep, capacity, share), jnp.bfloat16),
+            jax.ShapeDtypeStruct((rows, model), jnp.bfloat16),
+        ),
+        in_specs=[pl.BlockSpec(memory_space=pltpu.VMEM)] * 2,
+        out_specs=[pl.BlockSpec(memory_space=pltpu.VMEM)] * 2,
+        scratch_shapes=[held(n_ep, n_y, capacity, share)] * 3
+        + [held(n_ep, capacity, share)]
+        + [held(n_y, rows, model)] * 3
+        + [pltpu.SemaphoreType.DMA((1,))]
+        + [many] * 4
+        + [one] * 2
+        + [few] * 4,
+        compiler_params=pltpu.CompilerParams(collective_id=1, has_side_effects=True),
+    )(partial_rows, projected)
+
+
+def mixer_scan(
     receptance,
     key_matrix,
     value_matrix,
@@ -236,7 +550,6 @@
     correction_rate_offset,
     extra_head_log_decay,
     head_norm_gain,
-    mixer_output_weight,
 ):
     positions, own_width = receptance.shape
     pairs = -(-own_width // PAIR)
@@ -245,7 +558,6 @@
     def filled(x, columns=width):
         return x if x.shape[-1] == columns else jnp.pad(x, ((0, 0), (0, columns - x.shape[-1])))
 
-    whole_weight = lax.all_gather(mixer_output_weight, "tp", axis=0, tiled=True)
     blocks = positions // HEAD_DIM
     group = 4 if blocks % 4 == 0 else 1
     local, reach, ends = pl.pallas_call(
@@ -269,40 +581,31 @@
         filled(correction_rate_offset[None]),
         filled(extra_head_log_decay, 2 * pairs),
     )
-    everyone = lax.all_gather(ends, "ep")
+    return local, reach, ends, filled(output_gate_input), filled(head_norm_gain[None])
+
+
+def mixer_finish(everyone, local, reach, gate_input, gain, mixer_output_weight):
+    positions, width = local.shape
+    own_width = mixer_output_weight.shape[0]
     mixed_hidden = pl.pallas_call(
         functools.partial(join_kernel, "ep"),
         out_shape=jax.ShapeDtypeStruct((positions, width), jnp.bfloat16),
         cost_estimate=pl.CostEstimate(
             flops=6000 * positions * width, bytes_accessed=16 * positions * width, transcendentals=0
         ),
-    )(everyone, local, reach, filled(output_gate_input), filled(head_norm_gain[None]))
+    )(everyone, local, reach, gate_input, gain)
     mixed_hidden = mixed_hidden[:, :own_width]
-    own_rows = lax.all_to_all(mixed_hidden, "tp", split_axis=0, concat_axis=1, tiled=True)
-    return jnp.dot(own_rows, whole_weight, preferred_element_type=jnp.float32).astype(jnp.bfloat16)
-
-
-def finish_experts(gate_val, up_val, expert_down_weight):
-    expert_hidden = (jax.nn.silu(gate_val) * up_val).astype(jnp.bfloat16)
-    return lax.psum_scatter(
-        jnp.einsum(
-            "sxcf,xfd->dsxc", expert_hidden, expert_down_weight, preferred_element_type=jnp.float32
-        ).astype(jnp.bfloat16),
-        "tp",
-        scatter_dimension=0,
-        tiled=True,
-    )
-
-
-def expert_part(
+    return jnp.dot(mixed_hidden, mixer_output_weight, preferred_element_type=jnp.float32).astype(
+        jnp.bfloat16
+    )
+
+
+def expert_route(
     expert_layer_input,
     feedforward_norm_gain,
     group_router_weight,
     expert_router_weight,
     routes,
-    expert_gate_weight,
-    expert_up_weight,
-    expert_down_weight,
 ):
     token_rows = expert_layer_input.shape[0]
     route_count = routes.shape[1]
@@ -341,28 +644,29 @@
     outgoing = jnp.dot(dispatch_matrix, normed_input, preferred_element_type=jnp.float32).astype(
         jnp.bfloat16
     )
-    outgoing = outgoing.reshape(ep_count, expert_total // ep_count, capacity, outgoing.shape[1])
-    width_share = outgoing.shape[3] // lax.axis_size("tp")
+    outgoing = outgoing.reshape(ep_count, capacity, outgoing.shape[1])
+    width_share = outgoing.shape[2] // lax.axis_size("tp")
     own_columns = lax.dynamic_slice_in_dim(
-        outgoing, lax.axis_index("tp") * width_share, width_share, 3
-    )
-    piece = lax.all_gather(
-        lax.all_to_all(own_columns, "ep", split_axis=0, concat_axis=0, tiled=True),
-        "tp",
-        axis=3,
-        tiled=True,
-    )
-    gate_val = jnp.einsum(
-        "sxcd,xdf->sxcf", piece, expert_gate_weight, preferred_element_type=jnp.float32
-    )
-    up_val = jnp.einsum(
-        "sxcd,xdf->sxcf", piece, expert_up_weight, preferred_element_type=jnp.float32
-    )
-    expert_rows = finish_experts(gate_val, up_val, expert_down_weight)
-    homebound = lax.all_to_all(expert_rows, "ep", split_axis=1, concat_axis=1, tiled=True)
-    homebound = homebound.reshape(homebound.shape[0], expert_total * capacity)
-    combined = jnp.dot(homebound.astype(jnp.float32), combine_matrix, precision=highest)
-    return combined.T.astype(jnp.bfloat16)
+        outgoing, lax.axis_index("tp") * width_share, width_share, 2
+    )
+    return own_columns, combine_matrix
+
+
+def expert_rows(piece, expert_gate_weight, expert_up_weight, expert_down_weight):
+    rows = piece.reshape(-1, piece.shape[2])
+    gate_val = jnp.dot(rows, expert_gate_weight[0], preferred_element_type=jnp.float32)
+    up_val = jnp.dot(rows, expert_up_weight[0], preferred_element_type=jnp.float32)
+    expert_hidden = (jax.nn.silu(gate_val) * up_val).astype(jnp.bfloat16)
+    result = jnp.dot(expert_hidden, expert_down_weight[0], preferred_element_type=jnp.float32)
+    return result.astype(jnp.bfloat16).reshape(piece.shape)
+
+
+def expert_combine(homebound, combine_matrix):
+    homebound = homebound.reshape(-1, homebound.shape[2]).astype(jnp.float32)
+    combined = lax.dot_general(
+        combine_matrix, homebound, (((0,), (0,)), ((), ())), precision=highest
+    )
+    return combined.astype(jnp.bfloat16)
 
 
 def local(
@@ -386,7 +690,7 @@
     expert_up_weight,
     expert_down_weight,
 ):
-    token_mixer_output = mixer_part(
+    local_read, reach, ends, gate_input, gain = mixer_scan(
         receptance,
         key_matrix,
         value_matrix,
@@ -397,19 +701,19 @@
         correction_rate_offset,
         extra_head_log_decay,
         head_norm_gain,
-        mixer_output_weight,
-    )
-    expert_out = expert_part(
+    )
+    own_columns, combine_matrix = expert_route(
         expert_layer_input,
         feedforward_norm_gain,
         group_router_weight,
         expert_router_weight,
         routes,
-        expert_gate_weight,
-        expert_up_weight,
-        expert_down_weight,
-    )
-    return (token_mixer_output, expert_out)
+    )
+    piece, everyone = exchange_out(own_columns, ends)
+    projected = mixer_finish(everyone, local_read, reach, gate_input, gain, mixer_output_weight)
+    partial_rows = expert_rows(piece, expert_gate_weight, expert_up_weight, expert_down_weight)
+    homebound, token_mixer_output = exchange_back(partial_rows, projected)
+    return (token_mixer_output, expert_combine(homebound, combine_matrix))
 
 
 def solution(mesh):

time: 164 us -> 112 us (0.68)
  Pallas kernels: 11.4 us -> 80.2 us
  blocking collectives: 55.2 us -> 0 us
  waiting for transfers between devices: 41.5 us -> 0 us
  between operations: 13.9 us -> 0.8 us
  starting transfers between devices: 10.4 us -> 0 us
    pallas_call x2 -> x4, Pallas kernels: 11.4 us -> 80.2 us  [the longest x1 38.8 us: exchange_back(): pl.pallas_call(return_kernel, out_shape=(jax.ShapeDtypeStruct((n_ep, capa...]
    all_gather x1 -> x0, blocking collectives: 33.5 us -> none  [mixer_part(): everyone = lax.all_gather(ends, 'ep')]
    all_gather x2 -> x0, waiting for transfers between devices: 23.9 us -> none  [the longest x1 21.7 us: expert_part(): lax.all_gather(lax.all_to_all(own_columns, 'ep', split_axis=0, concat_axi...]
    all_to_all x1 -> x0, blocking collectives: 21.7 us -> none  [expert_part(): lax.all_to_all(own_columns, 'ep', split_axis=0, concat_axis=0, tiled=True)]
    all_to_all x2 -> x0, waiting for transfers between devices: 16.8 us -> none  [the longest x1 8.51 us: mixer_part(): lax.all_to_all(mixed_hidden, 'tp', split_axis=0, concat_axis=1, tiled=True)]
    all_to_all x2 -> x0, starting transfers between devices: 10.3 us -> none  [the longest x1 6.88 us: expert_part(): lax.all_to_all(expert_rows, 'ep', split_axis=1, concat_axis=1, tiled=True)]
    all_to_all x1 -> x0, local copies, waits for them, and re-layouts: 1.8 us -> none  [mixer_part(): lax.all_to_all(mixed_hidden, 'tp', split_axis=0, concat_axis=1, tiled=True)]
  transfers between devices with their start and end apart: 5 -> 0, of which waited for: 4 -> 0; matrix products, arithmetic and copies ran while one was open for 4% -> 0% of each run, Pallas kernels for 7% -> 0%
where the time goes in v2:
time: 112 us; the launch traced here: 111 us
  Pallas kernels  80.2 us (72%)
  matrix products  23.1 us (21%)
  local copies, waits for them, and re-layouts  4.3 us (4%)
  other arithmetic  2.88 us (3%)
    pallas_call x1, Pallas kernels, exchange_back(): pl.pallas_call(return_kernel, out_shape=(jax.ShapeDtypeStruct((n_ep, capa...  38.8 us
    pallas_call x1, Pallas kernels, exchange_out(): pl.pallas_call(dispatch_kernel, out_shape=(jax.ShapeDtypeStruct((n_ep, ca...  30 us
    dot_general x1, matrix products, expert_rows(): jnp.dot(expert_hidden, expert_down_weight[0], preferred_element_type=jnp....  9.98 us
    pallas_call x1, Pallas kernels, mixer_scan(): pl.pallas_call(functools.partial(scan_kernel, group), out_shape=(jax.Shap...  8.48 us
    dot_general x1, matrix products, expert_rows(): jnp.dot(rows, expert_gate_weight[0], preferred_element_type=jnp.float32)  6.59 us
    dot_general x1, matrix products, mixer_finish(): jnp.dot(mixed_hidden, mixer_output_weight, preferred_element_type=jnp.flo...  2.96 us
    pallas_call x1, Pallas kernels, mixer_finish(): pl.pallas_call(functools.partial(join_kernel, 'ep'), out_shape=jax.ShapeD...  2.93 us
    unnamed x23, local copies, waits for them, and re-layouts  2.73 us

profile of v2, /device:TPU:0, one launch (start us, length us, event | category | flops | bytes accessed | tf_op | source)
XLA Modules:
  0.0 111.3 jit_solution(5328176223869584516)
XLA Ops:
  0.6 0.0 copy-start
  0.6 0.9 copy.42
  1.5 0.1 eq.64
  1.7 0.6 reduce-window.6
  2.3 0.2 slice_reduce_fusion
  2.5 0.1 eq.60
  2.7 0.1 fusion.18
  2.8 0.1 reduce_sum.57
  2.9 0.1 copy.44
  3.0 0.7 and_select_fusion
  3.7 0.1 fusion.16
  3.7 0.0 copy-start.6
  3.7 1.2 %fusion.11 = f32[128]{0:T(128)S(1)} fusion(bf16[128,2048]{1,0:T(8,128)(2,1)} %param.30), kind=kLoop, calls=%fused_computation.14 | loop fusion | flops 786304 | bytes 524800 | tf_op jit(solution)/shard_map/reduce_sum | solution.py:619
  5.0 1.8 %convolution_convert_fusion.1 = bf16[512,2048]{1,0:T(8,128)(2,1)S(1)} fusion(pred[512,128]{1,0:T(8,128)(4,1)S(1)} %fusion.16, bf16[128,2048]{1,0:T(8,128)(2,1)} %param.30, f32[2048]{0:T(1024)} %param.31, f32[128]{0:T(128)S(1)} %add_rsqrt_fusion), kind=kOutput, calls=%fused_computation.8 | convolution fusion | flops 270532608 | bytes 2695680 | tf_op jit(solution)/shard_map/dot_general | solution.py:644
  6.8 0.8 constant_dynamic-slice_fusion.cols_ref
  7.7 0.0 copy-done.6
  7.7 0.9 copy.45.extra_ref
  8.5 8.5 %shard_map.194 = (f32[512,256]{1,0:T(8,128)}, bf16[512,256]{1,0:T(8,128)(2,1)}, bf16[256,128]{1,0:T(8,128)(2,1)}) custom-call(bf16[512,256]{1,0:T(8,128)(2,1)} %r_ref.1, bf16[512,256]{1,0:T(8,128)(2,1)} %k_ref.1, bf16[512,256]{1,0:T(8,128)(2,1)} %v_ref.1, bf16[512,256]{1,0:T(8,128)(2,1)} %d_ref.1, bf16[512,256]{1,0:T(8,128)(2,1)} %a_ref.1, ...), custom_call_target="tpu_custom_call" | custom-call | flops 7864320000 | bytes 2097152 | tf_op jit(solution)/shard_map/pallas_call | solution.py:563
  17.0 30.0 %shard_map.195 = (bf16[8,64,2048]{2,1,0:T(8,128)(2,1)}, bf16[8,256,128]{2,1,0:T(8,128)(2,1)}) custom-call(bf16[8,64,512]{2,1,0:T(8,128)(2,1)} %constant_dynamic-slice_fusion.cols_ref, bf16[256,128]{1,0:T(8,128)(2,1)} %get-tuple-element.9.ends_ref), custom_call_target="tpu_custom_call" | custom-call | tf_op jit(solution)/shard_map/pallas_call | solution.py:499
  47.1 0.0 copy-start.7
  47.1 6.6 %fusion.4 = f32[512,1024]{1,0:T(8,128)} fusion(bf16[512,2048]{1,0:T(8,128)(2,1)} %bitcast.42, bf16[1,2048,1024]{2,1,0:T(8,128)(2,1)} %param.35), kind=kOutput, calls=%fused_computation.4 | convolution fusion | flops 2147483648 | bytes 8388608 | tf_op jit(solution)/shard_map/dot_general | solution.py:657
  53.7 0.0 copy-done.7
  53.7 10.0 %fusion.6 = bf16[512,2048]{1,0:T(8,128)(2,1)} fusion(bf16[1,1024,2048]{2,1,0:T(8,128)(2,1)} %param.37, f32[512,1024]{1,0:T(8,128)} %fusion.4, bf16[512,2048]{1,0:T(8,128)(2,1)S(1)} %bitcast.43, bf16[1,2048,1024]{2,1,0:T(8,128)(2,1)} %param.36), kind=kOutput, calls=%fused_computation.6 | convolution fusion | flops 4299161600 | bytes 14680064 | tf_op jit(solution)/shard_map/dot_general | solution.py:660
  63.6 2.9 %shard_map.196 = bf16[512,256]{1,0:T(8,128)(2,1)} custom-call(bf16[8,256,128]{2,1,0:T(8,128)(2,1)} %get-tuple-element.11.all_ref, f32[512,256]{1,0:T(8,128)} %get-tuple-element.12.out_ref, bf16[512,256]{1,0:T(8,128)(2,1)} %get-tuple-element.13.reach_ref, bf16[512,256]{1,0:T(8,128)(2,1)} %gate_ref.1, f32[1,256]{1,0:T(1,128)} %bitcast.46), custom_call_target="tpu_custom_call" | custom-call | flops 786432000 | bytes 2097152 | tf_op jit(solution)/shard_map/pallas_call | solution.py:590
  66.6 0.0 copy-done
  66.6 3.0 %convolution_convert_fusion.proj_ref = bf16[512,2048]{1,0:T(8,128)(2,1)} fusion(bf16[512,256]{1,0:T(8,128)(2,1)} %shard_map.196, bf16[256,2048]{1,0:T(8,128)(2,1)S(1)} %copy-done), kind=kOutput, calls=%fused_computation.7 | convolution fusion | flops 537919488 | bytes 3407872 | tf_op jit(solution)/shard_map/dot_general | solution.py:598
  69.5 0.0 copy-start.1
  69.5 0.0 copy-start.5
  69.5 0.0 copy-start.9
  69.5 0.0 copy-start.8
  69.5 0.0 copy-start.4
  69.6 38.8 %shard_map.197 = (bf16[8,64,512]{2,1,0:T(8,128)(2,1)}, bf16[128,2048]{1,0:T(8,128)(2,1)}) custom-call(bf16[8,64,2048]{2,1,0:T(8,128)(2,1)} %bitcast.40, bf16[512,2048]{1,0:T(8,128)(2,1)} %convolution_convert_fusion.proj_ref), custom_call_target="tpu_custom_call" | custom-call | tf_op jit(solution)/shard_map/pallas_call | solution.py:523
  108.3 0.0 copy-start.2
  108.3 0.0 copy-start.3
  108.3 0.0 copy-done.1
  108.4 0.0 copy-done.5
  108.4 0.0 copy-done.9
  108.4 0.3 fusion.25
  108.7 0.0 copy-done.8
  108.8 0.3 fusion.21
  109.1 0.0 copy-done.4
  109.1 0.1 select_reduce_fusion
  109.2 0.1 copy-done.2
  109.4 1.1 %convolution_convert_fusion.2 = bf16[128,512]{1,0:T(8,128)(2,1)} fusion(f32[512,128]{1,0:T(8,128)S(1)} %select_reduce_fusion, bf16[512,512]{1,0:T(8,128)(2,1)S(1)} %bitcast.41), kind=kOutput, calls=%fused_computation.12 | convolution fusion | flops 402718720 | bytes 917504 | tf_op jit(solution)/shard_map/dot_general | solution.py:666
  110.5 0.0 copy-done.3
  110.5 0.8 copy.47
  (9 shorter events, 0.2 us)
Async XLA Ops:
  0.6 65.9 %copy-start = (bf16[256,2048]{1,0:T(8,128)(2,1)S(1)}, bf16[256,2048]{1,0:T(8,128)(2,1)}, u32[]{:S(2)}) copy-start(bf16[256,2048]{1,0:T(8,128)(2,1)} %param.29) | copy-start | bytes 3145732
  3.7 3.9 %copy-start.6 = (f32[512,4]{0,1:T(4,128)S(1)}, f32[512,4]{0,1:T(4,128)}, u32[]{:S(2)}) copy-start(f32[512,4]{0,1:T(4,128)} %param.27) | copy-start | bytes 24580
  47.1 6.6 %copy-start.7 = (bf16[8,64,2048]{2,1,0:T(8,128)(2,1)S(1)}, bf16[8,64,2048]{2,1,0:T(8,128)(2,1)}, u32[]{:S(2)}) copy-start(bf16[8,64,2048]{2,1,0:T(8,128)(2,1)} %get-tuple-element.10) | copy-start | bytes 6291460
  69.5 38.8 %copy-start.1 = (bf16[128,2048]{1,0:T(8,128)(2,1)S(1)}, bf16[128,2048]{1,0:T(8,128)(2,1)}, u32[]{:S(2)}) copy-start(bf16[128,2048]{1,0:T(8,128)(2,1)} %param.30) | copy-start | bytes 1572868
  69.5 38.8 %copy-start.5 = (f32[2048]{0:T(1024)S(1)}, f32[2048]{0:T(1024)}, u32[]{:S(2)}) copy-start(f32[2048]{0:T(1024)} %param.31) | copy-start | bytes 24580
  69.5 38.8 %copy-start.9 = (bf16[2048,4]{0,1:T(4,128)(2,1)S(1)}, bf16[2048,4]{0,1:T(4,128)(2,1)}, u32[]{:S(2)}) copy-start(bf16[2048,4]{0,1:T(4,128)(2,1)} %param.32) | copy-start | bytes 49156
  69.5 39.2 %copy-start.8 = (bf16[2048,8]{0,1:T(8,128)(2,1)S(1)}, bf16[2048,8]{0,1:T(8,128)(2,1)}, u32[]{:S(2)}) copy-start(bf16[2048,8]{0,1:T(8,128)(2,1)} %param.33) | copy-start | bytes 98308
  69.5 39.5 %copy-start.4 = (s32[128,2]{0,1:T(2,128)S(1)}, s32[128,2]{0,1:T(2,128)}, u32[]{:S(2)}) copy-start(s32[128,2]{0,1:T(2,128)} %param.34) | copy-start | bytes 3076
  108.3 1.0 copy-start.2
  108.3 2.2 %copy-start.3 = (bf16[128,2048]{1,0:T(8,128)(2,1)S(1)}, bf16[128,2048]{1,0:T(8,128)(2,1)}, u32[]{:S(2)}) copy-start(bf16[128,2048]{1,0:T(8,128)(2,1)} %get-tuple-element.22) | copy-start | bytes 1572868

commit v3 on v2

--- a/solution.py
+++ b/solution.py
@@ -261,7 +261,33 @@
 
 
 def dispatch_kernel(
-    cols_ref, ends_ref, piece_ref, every_ref, own_sem, es, er, gs, gr, cs, cr, ys, yr, fs, fr
+    group,
+    r_ref,
+    k_ref,
+    v_ref,
+    d_ref,
+    a_ref,
+    d_off_ref,
+    a_off_ref,
+    extra_ref,
+    cols_ref,
+    out_ref,
+    reach_ref,
+    piece_ref,
+    every_ref,
+    chain_ref,
+    ends_ref,
+    own_sem,
+    es,
+    er,
+    gs,
+    gr,
+    cs,
+    cr,
+    ys,
+    yr,
+    fs,
+    fr,
 ):
     n_ep, n_tp, n_y, e, t, y, core = place_of()
     share = cols_ref.shape[2]
@@ -277,7 +303,6 @@
     own = pltpu.make_async_copy(cols_ref.at[e], block(e, t), own_sem.at[0])
     own_ends = pltpu.make_async_copy(ends_ref, every_ref.at[e], own_sem.at[1])
     own.start()
-    own_ends.start()
 
     def ep_copy(d):
         peer = lax.rem(e + d, n_ep)
@@ -311,7 +336,6 @@
         lax.fori_loop(first, n_ep, run, 0)
 
     every(1, lambda d: ep_copy(d).start())
-    every(1, lambda d: ends_copy(d).start())
 
     def share_out(d):
         core_copy(d).start()
@@ -320,12 +344,29 @@
 
     own.wait()
     share_out(0)
+    scan_kernel(
+        group,
+        r_ref,
+        k_ref,
+        v_ref,
+        d_ref,
+        a_ref,
+        d_off_ref,
+        a_off_ref,
+        extra_ref,
+        out_ref,
+        reach_ref,
+        ends_ref,
+        chain_ref,
+    )
 
     def arrived(d):
         ep_copy(d).wait_recv()
         share_out(d)
 
     every(1, arrived)
+    every(1, lambda d: ends_copy(d).start())
+    own_ends.start()
 
     def pass_on(d):
         for h in range(1, n_y):
@@ -351,10 +392,19 @@
 
 
 def return_kernel(
-    part_ref,
+    piece_ref,
     proj_ref,
+    gate_hbm,
+    up_hbm,
+    down_hbm,
     home_ref,
     mixer_ref,
+    gate_ref,
+    up_ref,
+    down_ref,
+    rows_ref,
+    hidden_ref,
+    part_ref,
     near_ref,
     stage_ref,
     far_ref,
@@ -362,7 +412,9 @@
     mnear_ref,
     mstage_ref,
     mfar_ref,
-    own_sem,
+    gate_sem,
+    up_sem,
+    down_sem,
     ns,
     nr,
     ys,
@@ -375,15 +427,36 @@
     myr,
 ):
     n_ep, n_tp, n_y, e, t, y, core = place_of()
-    share = part_ref.shape[2] // n_tp
-    rows = proj_ref.shape[0] // n_tp
+    capacity, model = part_ref.shape[1:]
+    units = gate_ref.shape[1]
+    share = model // n_tp
+    rows = proj_ref.shape[0] // (2 * n_tp)
     other = 2 * y + 1 - core
+    half = n_ep // 2
+    wide_units, wide_model = min(256, units), min(512, model)
+
+    def gate_copy(i):
+        at = pl.ds(pl.multiple_of(i * wide_units, wide_units), wide_units)
+        return (
+            pltpu.make_async_copy(gate_hbm.at[0, :, at], gate_ref.at[:, at], gate_sem.at[i]),
+            pltpu.make_async_copy(up_hbm.at[0, :, at], up_ref.at[:, at], up_sem.at[i]),
+        )
+
+    def down_copy(i):
+        at = pl.ds(pl.multiple_of(i * wide_model, wide_model), wide_model)
+        return pltpu.make_async_copy(down_hbm.at[0, :, at], down_ref.at[:, at], down_sem.at[i])
+
+    for i in range(units // wide_units):
+        for copy in gate_copy(i):
+            copy.start()
+    for i in range(model // wide_model):
+        down_copy(i).start()
 
     def columns(index):
         return pl.ds(pl.multiple_of(index * share, share), share)
 
-    def row_block(index):
-        return pl.ds(pl.multiple_of(index * rows, rows), rows)
+    def row_block(index, q):
+        return pl.ds(pl.multiple_of((2 * index + q) * rows, rows), rows)
 
     def peer_y(h):
         return lax.rem(y + h, n_y)
@@ -397,62 +470,96 @@
             stage_ref.at[s, h], far_ref.at[s, h], ys.at[s, h], yr.at[s, h], e, 2 * peer_y(h) + core
         )
 
-    def home_of(d):
-        return lax.rem(e + d, n_ep)
-
-    def home_copy(d):
-        peer = home_of(d)
+    def offset(k):
+        m = lax.div(k + 1, 2)
+        return lax.rem(half + m * (2 * lax.rem(k, 2) - 1) + n_ep, n_ep)
+
+    def home_of(k):
+        return lax.rem(e + offset(k), n_ep)
+
+    def home_copy(k):
+        peer, d = home_of(k), offset(k)
         return remote(final_ref.at[peer], home_ref.at[e], es.at[d], er.at[d], peer, t)
 
-    def mnear_copy(h):
-        src = proj_ref.at[row_block(2 * peer_y(h) + 1 - core), :]
-        return remote(src, mnear_ref.at[h], mns.at[h], mnr.at[h], e, other)
-
-    def my_copy(h):
+    def mnear_copy(q, h):
+        src = proj_ref.at[row_block(2 * peer_y(h) + 1 - core, q), :]
+        return remote(src, mnear_ref.at[q, h], mns.at[q, h], mnr.at[q, h], e, other)
+
+    def my_copy(q, h):
+        target = 2 * peer_y(h) + core
         return remote(
-            mstage_ref.at[h], mfar_ref.at[h], mys.at[h], myr.at[h], e, 2 * peer_y(h) + core
+            mstage_ref.at[q, h], mfar_ref.at[q, h], mys.at[q, h], myr.at[q, h], e, target
         )
 
-    def every(first, body):
+    def span(first, last, body):
         def run(d, carry):
             body(d)
             return carry
 
-        lax.fori_loop(first, n_ep, run, 0)
-
-    meet()
-
-    def start_near(d):
-        for h in range(n_y):
-            near_copy(home_of(d), h).start()
-
-    every(1, start_near)
-    start_near(0)
-    for h in range(n_y):
-        mnear_copy(h).start()
+        lax.fori_loop(first, last, run, 0)
 
     def wide(x):
         return x.astype(jnp.float32)
 
+    def mixer_sum(q, h):
+        return wide(proj_ref[row_block(2 * peer_y(h) + core, q), :]) + wide(mnear_ref[q, h])
+
+    def mixer_share(q):
+        for h in range(1, n_y):
+            mnear_copy(q, h).wait_recv()
+            mstage_ref[q, h] = bf(mixer_sum(q, h))
+            my_copy(q, h).start()
+
+    def mixer_end(q):
+        mnear_copy(q, 0).wait_recv()
+        total = mixer_sum(q, 0)
+        for h in range(1, n_y):
+            my_copy(q, h).wait_recv()
+            total = total + wide(mfar_ref[q, h])
+        mixer_ref[q * rows : (q + 1) * rows] = bf(total)
+
+    def widen(b):
+        def take(k):
+            at = pl.ds(pl.multiple_of((k - b * half) * capacity, capacity), capacity)
+            rows_ref[at, :] = piece_ref[home_of(k)]
+
+        span(b * half, (b + 1) * half, take)
+
+        def unit_tile(i):
+            if b == 0:
+                for copy in gate_copy(i):
+                    copy.wait()
+            at = pl.ds(pl.multiple_of(i * wide_units, wide_units), wide_units)
+            x = rows_ref[...]
+            gate_val = mm(x, gate_ref[:, at])
+            hidden_ref[:, at] = bf(gate_val * logistic(gate_val) * mm(x, up_ref[:, at]))
+
+        span(0, units // wide_units, unit_tile)
+
+    def narrow(b):
+        def model_tile(i):
+            if b == 0:
+                down_copy(i).wait()
+            at = pl.ds(pl.multiple_of(i * wide_model, wide_model), wide_model)
+            result = bf(mm(hidden_ref[...], down_ref[:, at]))
+            for j in range(half):
+                part_ref[home_of(b * half + j), :, at] = result[j * capacity : (j + 1) * capacity]
+
+        span(0, model // wide_model, model_tile)
+
+    def start_near(k):
+        for h in range(n_y):
+            near_copy(home_of(k), h).start()
+
     def pair_sum(s, h):
         return wide(part_ref[s, :, columns(2 * peer_y(h) + core)]) + wide(near_ref[s, h])
 
-    def add_near(s):
+    def add_near(k):
+        s = home_of(k)
         for h in range(1, n_y):
             near_copy(s, h).wait_recv()
             stage_ref[s, h] = bf(pair_sum(s, h))
             y_copy(s, h).start()
-
-    every(1, lambda d: add_near(home_of(d)))
-    add_near(e)
-
-    def mixer_sum(h):
-        return wide(proj_ref[row_block(2 * peer_y(h) + core), :]) + wide(mnear_ref[h])
-
-    for h in range(1, n_y):
-        mnear_copy(h).wait_recv()
-        mstage_ref[h] = bf(mixer_sum(h))
-        my_copy(h).start()
 
     def add_far(s):
         near_copy(s, 0).wait_recv()
@@ -462,20 +569,30 @@
             total = total + wide(far_ref[s, h])
         return bf(total)
 
-    def go_home(d):
-        s = home_of(d)
+    def go_home(k):
+        s = home_of(k)
         final_ref[s] = add_far(s)
-        home_copy(d).start()
-
-    every(1, go_home)
+        home_copy(k).start()
+
+    meet()
+    for q in range(2):
+        for h in range(n_y):
+            mnear_copy(q, h).start()
+    mixer_share(0)
+    widen(0)
+    narrow(0)
+    span(0, half, start_near)
+    widen(1)
+    span(0, half, add_near)
+    narrow(1)
+    span(half, n_ep, start_near)
+    span(half, n_ep, add_near)
+    mixer_share(1)
+    span(0, half, go_home)
+    mixer_end(0)
+    span(half, n_ep - 1, go_home)
     home_ref[e] = add_far(e)
-
-    mnear_copy(0).wait_recv()
-    total = mixer_sum(0)
-    for h in range(1, n_y):
-        my_copy(h).wait_recv()
-        total = total + wide(mfar_ref[h])
-    mixer_ref[...] = bf(total)
+    mixer_end(1)
 
     def close(s):
         for h in range(n_y):
@@ -483,63 +600,58 @@
         for h in range(1, n_y):
             y_copy(s, h).wait_send()
 
-    every(0, close)
-    for h in range(n_y):
-        mnear_copy(h).wait_send()
-    for h in range(1, n_y):
-        my_copy(h).wait_send()
-    every(1, lambda d: home_copy(d).wait())
-
-
-def exchange_out(own_columns, ends):
+    span(0, n_ep, close)
+    for q in range(2):
+        for h in range(n_y):
+            mnear_copy(q, h).wait_send()
+        for h in range(1, n_y):
+            my_copy(q, h).wait_send()
+    span(0, n_ep - 1, lambda k: home_copy(k).wait())
+
+
+def experts_and_back(piece, projected, gate_weight, up_weight, down_weight):
     n_ep, n_tp = lax.axis_size("ep"), lax.axis_size("tp")
     n_y = n_tp // 2
-    capacity, share = own_columns.shape[1:]
-    one, many = pltpu.SemaphoreType.DMA((n_ep,)), pltpu.SemaphoreType.DMA((n_y, n_ep))
-    return pl.pallas_call(
-        dispatch_kernel,
-        out_shape=(
-            jax.ShapeDtypeStruct((n_ep, capacity, n_tp * share), jnp.bfloat16),
-            jax.ShapeDtypeStruct((n_ep, *ends.shape), jnp.bfloat16),
-        ),
-        in_specs=[pl.BlockSpec(memory_space=pltpu.VMEM)] * 2,
-        out_specs=[pl.BlockSpec(memory_space=pltpu.VMEM)] * 2,
-        scratch_shapes=[pltpu.SemaphoreType.DMA((2,))] + [one] * 6 + [many] * 4,
-        compiler_params=pltpu.CompilerParams(collective_id=0, has_side_effects=True),
-    )(own_columns, ends)
-
-
-def exchange_back(partial_rows, projected):
-    n_ep, n_tp = lax.axis_size("ep"), lax.axis_size("tp")
-    n_y = n_tp // 2
-    capacity, model = partial_rows.shape[1:]
+    capacity, model = piece.shape[1:]
+    units = gate_weight.shape[2]
     share, rows = model // n_tp, projected.shape[0] // n_tp
-    many, few = pltpu.SemaphoreType.DMA((n_ep, n_y)), pltpu.SemaphoreType.DMA((n_y,))
+    many, few = pltpu.SemaphoreType.DMA((n_ep, n_y)), pltpu.SemaphoreType.DMA((2, n_y))
     one = pltpu.SemaphoreType.DMA((n_ep,))
 
     def held(*shape):
         return pltpu.VMEM(shape, jnp.bfloat16)
 
+    in_vmem = pl.BlockSpec(memory_space=pltpu.VMEM)
     return pl.pallas_call(
         return_kernel,
         out_shape=(
             jax.ShapeDtypeStruct((n_ep, capacity, share), jnp.bfloat16),
             jax.ShapeDtypeStruct((rows, model), jnp.bfloat16),
         ),
-        in_specs=[pl.BlockSpec(memory_space=pltpu.VMEM)] * 2,
-        out_specs=[pl.BlockSpec(memory_space=pltpu.VMEM)] * 2,
-        scratch_shapes=[held(n_ep, n_y, capacity, share)] * 3
+        in_specs=[in_vmem] * 2 + [pl.BlockSpec(memory_space=pl.ANY)] * 3,
+        out_specs=[in_vmem] * 2,
+        scratch_shapes=[
+            held(model, units),
+            held(model, units),
+            held(units, model),
+            held(n_ep // 2 * capacity, model),
+            held(n_ep // 2 * capacity, units),
+            held(n_ep, capacity, model),
+        ]
+        + [held(n_ep, n_y, capacity, share)] * 3
         + [held(n_ep, capacity, share)]
-        + [held(n_y, rows, model)] * 3
-        + [pltpu.SemaphoreType.DMA((1,))]
+        + [held(2, n_y, rows // 2, model)] * 3
+        + [pltpu.SemaphoreType.DMA((max(1, units // 256),))] * 2
+        + [pltpu.SemaphoreType.DMA((max(1, model // 512),))]
         + [many] * 4
         + [one] * 2
         + [few] * 4,
         compiler_params=pltpu.CompilerParams(collective_id=1, has_side_effects=True),
-    )(partial_rows, projected)
-
-
-def mixer_scan(
+    )(piece, projected, gate_weight, up_weight, down_weight)
+
+
+def scan_and_dispatch(
+    own_columns,
     receptance,
     key_matrix,
     value_matrix,
@@ -560,17 +672,29 @@
 
     blocks = positions // HEAD_DIM
     group = 4 if blocks % 4 == 0 else 1
-    local, reach, ends = pl.pallas_call(
-        functools.partial(scan_kernel, group),
+    n_ep, n_tp = lax.axis_size("ep"), lax.axis_size("tp")
+    n_y = n_tp // 2
+    capacity, share = own_columns.shape[1:]
+    ends = (pairs * 2 * HEAD_DIM, PAIR)
+    one, many = pltpu.SemaphoreType.DMA((n_ep,)), pltpu.SemaphoreType.DMA((n_y, n_ep))
+    local, reach, piece, everyone = pl.pallas_call(
+        functools.partial(dispatch_kernel, group),
         out_shape=(
             jax.ShapeDtypeStruct((positions, width), jnp.float32),
             jax.ShapeDtypeStruct((positions, width), jnp.bfloat16),
-            jax.ShapeDtypeStruct((pairs * 2 * HEAD_DIM, PAIR), jnp.bfloat16),
+            jax.ShapeDtypeStruct((n_ep, capacity, n_tp * share), jnp.bfloat16),
+            jax.ShapeDtypeStruct((n_ep, *ends), jnp.bfloat16),
         ),
-        scratch_shapes=[pltpu.VMEM((pairs, 2 * PAIR, PAIR), jnp.float32)],
-        cost_estimate=pl.CostEstimate(
-            flops=60000 * positions * width, bytes_accessed=16 * positions * width, transcendentals=0
-        ),
+        in_specs=[pl.BlockSpec(memory_space=pltpu.VMEM)] * 9,
+        out_specs=[pl.BlockSpec(memory_space=pltpu.VMEM)] * 4,
+        scratch_shapes=[
+            pltpu.VMEM((pairs, 2 * PAIR, PAIR), jnp.float32),
+            pltpu.VMEM(ends, jnp.bfloat16),
+            pltpu.SemaphoreType.DMA((2,)),
+        ]
+        + [one] * 6
+        + [many] * 4,
+        compiler_params=pltpu.CompilerParams(collective_id=0, has_side_effects=True),
     )(
         filled(receptance),
         filled(key_matrix),
@@ -580,8 +704,10 @@
         filled(decay_channel_offset[None]),
         filled(correction_rate_offset[None]),
         filled(extra_head_log_decay, 2 * pairs),
-    )
-    return local, reach, ends, filled(output_gate_input), filled(head_norm_gain[None])
+        own_columns,
+    )
+    gate_input, gain = filled(output_gate_input), filled(head_norm_gain[None])
+    return local, reach, piece, everyone, gate_input, gain
 
 
 def mixer_finish(everyone, local, reach, gate_input, gain, mixer_output_weight):
@@ -652,15 +778,6 @@
     return own_columns, combine_matrix
 
 
-def expert_rows(piece, expert_gate_weight, expert_up_weight, expert_down_weight):
-    rows = piece.reshape(-1, piece.shape[2])
-    gate_val = jnp.dot(rows, expert_gate_weight[0], preferred_element_type=jnp.float32)
-    up_val = jnp.dot(rows, expert_up_weight[0], preferred_element_type=jnp.float32)
-    expert_hidden = (jax.nn.silu(gate_val) * up_val).astype(jnp.bfloat16)
-    result = jnp.dot(expert_hidden, expert_down_weight[0], preferred_element_type=jnp.float32)
-    return result.astype(jnp.bfloat16).reshape(piece.shape)
-
-
 def expert_combine(homebound, combine_matrix):
     homebound = homebound.reshape(-1, homebound.shape[2]).astype(jnp.float32)
     combined = lax.dot_general(
@@ -690,7 +807,15 @@
     expert_up_weight,
     expert_down_weight,
 ):
-    local_read, reach, ends, gate_input, gain = mixer_scan(
+    own_columns, combine_matrix = expert_route(
+        expert_layer_input,
+        feedforward_norm_gain,
+        group_router_weight,
+        expert_router_weight,
+        routes,
+    )
+    local_read, reach, piece, everyone, gate_input, gain = scan_and_dispatch(
+        own_columns,
         receptance,
         key_matrix,
         value_matrix,
@@ -702,17 +827,10 @@
         extra_head_log_decay,
         head_norm_gain,
     )
-    own_columns, combine_matrix = expert_route(
-        expert_layer_input,
-        feedforward_norm_gain,
-        group_router_weight,
-        expert_router_weight,
-        routes,
-    )
-    piece, everyone = exchange_out(own_columns, ends)
     projected = mixer_finish(everyone, local_read, reach, gate_input, gain, mixer_output_weight)
-    partial_rows = expert_rows(piece, expert_gate_weight, expert_up_weight, expert_down_weight)
-    homebound, token_mixer_output = exchange_back(partial_rows, projected)
+    homebound, token_mixer_output = experts_and_back(
+        piece, projected, expert_gate_weight, expert_up_weight, expert_down_weight
+    )
     return (token_mixer_output, expert_combine(homebound, combine_matrix))
 
 

time: 112 us -> 91.6 us (0.82)
  matrix products: 23.1 us -> 6.54 us
  Pallas kernels: 80.2 us -> 76.8 us
    dot_general x2 -> x0, matrix products: 16.6 us -> none  [the longest x1 9.98 us: expert_rows(): jnp.dot(expert_hidden, expert_down_weight[0], preferred_element_type=jnp....]
    pallas_call x3 -> x2, Pallas kernels: 77.3 us -> 73.9 us  [the longest x1 41.3 us: experts_and_back(): pl.pallas_call(return_kernel, out_shape=(jax.ShapeDtypeStruct((n_ep, capa...]
    unnamed x23 -> x21, local copies, waits for them, and re-layouts: 2.73 us -> 2.73 us
where the time goes in v3:
time: 91.6 us; the launch traced here: 91.3 us
  Pallas kernels  76.8 us (84%)
  matrix products  6.54 us (7%)
  local copies, waits for them, and re-layouts  4.3 us (5%)
  other arithmetic  2.88 us (3%)
    pallas_call x1, Pallas kernels, experts_and_back(): pl.pallas_call(return_kernel, out_shape=(jax.ShapeDtypeStruct((n_ep, capa...  41.3 us
    pallas_call x1, Pallas kernels, scan_and_dispatch(): pl.pallas_call(functools.partial(dispatch_kernel, group), out_shape=(jax....  32.5 us
    dot_general x1, matrix products, mixer_finish(): jnp.dot(mixed_hidden, mixer_output_weight, preferred_element_type=jnp.flo...  2.96 us
    pallas_call x1, Pallas kernels, mixer_finish(): pl.pallas_call(functools.partial(join_kernel, 'ep'), out_shape=jax.ShapeD...  2.93 us
    unnamed x21, local copies, waits for them, and re-layouts  2.73 us

profile of v3, /device:TPU:0, one launch (start us, length us, event | category | flops | bytes accessed | tf_op | source)
XLA Modules:
  0.0 91.3 jit_solution(11875352695378742772)
XLA Ops:
  0.6 0.0 copy-start
  0.6 0.9 copy.42
  1.5 0.1 eq.64
  1.7 0.6 reduce-window.6
  2.3 0.2 slice_reduce_fusion
  2.5 0.1 eq.60
  2.7 0.1 fusion.5
  2.8 0.1 reduce_sum.57
  2.9 0.1 copy.44
  3.0 0.7 and_select_fusion
  3.7 0.1 fusion.3
  3.7 0.0 copy-start.6
  3.7 1.2 %fusion = f32[128]{0:T(128)S(1)} fusion(bf16[128,2048]{1,0:T(8,128)(2,1)} %param.30), kind=kLoop, calls=%fused_computation.6 | loop fusion | flops 786304 | bytes 524800 | tf_op jit(solution)/shard_map/reduce_sum | solution.py:745
  5.0 1.8 %convolution_convert_fusion.1 = bf16[512,2048]{1,0:T(8,128)(2,1)S(1)} fusion(pred[512,128]{1,0:T(8,128)(4,1)S(1)} %fusion.3, bf16[128,2048]{1,0:T(8,128)(2,1)} %param.30, f32[2048]{0:T(1024)} %param.31, f32[128]{0:T(128)S(1)} %add_rsqrt_fusion), kind=kOutput, calls=%fused_computation.1 | convolution fusion | flops 270532608 | bytes 2695680 | tf_op jit(solution)/shard_map/dot_general | solution.py:770
  6.8 0.8 constant_dynamic-slice_fusion.cols_ref
  7.7 0.0 copy-done.6
  7.7 0.9 copy.45.extra_ref
  8.5 32.5 %shard_map.194 = (f32[512,256]{1,0:T(8,128)}, bf16[512,256]{1,0:T(8,128)(2,1)}, bf16[8,64,2048]{2,1,0:T(8,128)(2,1)}, bf16[8,256,128]{2,1,0:T(8,128)(2,1)}) custom-call(bf16[512,256]{1,0:T(8,128)(2,1)} %r_ref.1, bf16[512,256]{1,0:T(8,128)(2,1)} %k_ref.1, bf16[512,256]{1,0:T(8,128)(2,1)} %v_ref.1, bf16[512,256]{1,0:T(8,128)(2,1)} %d_ref.1, ...), custom_call_target="tpu_custom_call" | custom-call | tf_op jit(solution)/shard_map/pallas_call | solution.py:680
  41.1 2.9 %shard_map.195 = bf16[512,256]{1,0:T(8,128)(2,1)} custom-call(bf16[8,256,128]{2,1,0:T(8,128)(2,1)} %get-tuple-element.9.all_ref, f32[512,256]{1,0:T(8,128)} %get-tuple-element.10.out_ref, bf16[512,256]{1,0:T(8,128)(2,1)} %get-tuple-element.11.reach_ref, bf16[512,256]{1,0:T(8,128)(2,1)} %gate_ref.1, f32[1,256]{1,0:T(1,128)} %bitcast.24), custom_call_target="tpu_custom_call" | custom-call | flops 786432000 | bytes 2097152 | tf_op jit(solution)/shard_map/pallas_call | solution.py:716
  44.0 0.0 copy-done
  44.0 3.0 %convolution_convert_fusion.proj_ref = bf16[512,2048]{1,0:T(8,128)(2,1)} fusion(bf16[512,256]{1,0:T(8,128)(2,1)} %shard_map.195, bf16[256,2048]{1,0:T(8,128)(2,1)S(1)} %copy-done), kind=kOutput, calls=%fused_computation | convolution fusion | flops 537919488 | bytes 3407872 | tf_op jit(solution)/shard_map/dot_general | solution.py:724
  47.0 0.0 copy-start.1
  47.0 0.0 copy-start.5
  47.0 0.0 copy-start.8
  47.0 0.0 copy-start.7
  47.0 0.0 copy-start.4
  47.0 41.3 %shard_map.196 = (bf16[8,64,512]{2,1,0:T(8,128)(2,1)}, bf16[128,2048]{1,0:T(8,128)(2,1)}) custom-call(bf16[8,64,2048]{2,1,0:T(8,128)(2,1)} %get-tuple-element.8.piece_ref, bf16[512,2048]{1,0:T(8,128)(2,1)} %convolution_convert_fusion.proj_ref, bf16[1,2048,1024]{2,1,0:T(8,128)(2,1)} %gate_hbm.1, bf16[1,2048,1024]{2,1,0:T(8,128)(2,1)} %up_hbm.1, ...), custom_call_target="tpu_custom_call" | custom-call | tf_op jit(solution)/shard_map/pallas_call | solution.py:625
  88.3 0.0 copy-start.2
  88.3 0.0 copy-start.3
  88.3 0.0 copy-done.1
  88.4 0.0 copy-done.5
  88.4 0.0 copy-done.8
  88.4 0.3 fusion.11
  88.7 0.0 copy-done.7
  88.8 0.3 fusion.7
  89.1 0.0 copy-done.4
  89.1 0.1 select_reduce_fusion
  89.2 0.1 copy-done.2
  89.4 1.1 %convolution_convert_fusion.2 = bf16[128,512]{1,0:T(8,128)(2,1)} fusion(f32[512,128]{1,0:T(8,128)S(1)} %select_reduce_fusion, bf16[512,512]{1,0:T(8,128)(2,1)S(1)} %bitcast.21), kind=kOutput, calls=%fused_computation.4 | convolution fusion | flops 402718720 | bytes 917504 | tf_op jit(solution)/shard_map/dot_general | solution.py:783
  90.5 0.0 copy-done.3
  90.5 0.8 copy.47
  (9 shorter events, 0.2 us)
Async XLA Ops:
  0.6 43.4 %copy-start = (bf16[256,2048]{1,0:T(8,128)(2,1)S(1)}, bf16[256,2048]{1,0:T(8,128)(2,1)}, u32[]{:S(2)}) copy-start(bf16[256,2048]{1,0:T(8,128)(2,1)} %param.29) | copy-start | bytes 3145732
  3.7 3.9 %copy-start.6 = (f32[512,4]{0,1:T(4,128)S(1)}, f32[512,4]{0,1:T(4,128)}, u32[]{:S(2)}) copy-start(f32[512,4]{0,1:T(4,128)} %param.27) | copy-start | bytes 24580
  47.0 41.4 %copy-start.1 = (bf16[128,2048]{1,0:T(8,128)(2,1)S(1)}, bf16[128,2048]{1,0:T(8,128)(2,1)}, u32[]{:S(2)}) copy-start(bf16[128,2048]{1,0:T(8,128)(2,1)} %param.30) | copy-start | bytes 1572868
  47.0 41.4 %copy-start.5 = (f32[2048]{0:T(1024)S(1)}, f32[2048]{0:T(1024)}, u32[]{:S(2)}) copy-start(f32[2048]{0:T(1024)} %param.31) | copy-start | bytes 24580
  47.0 41.4 %copy-start.8 = (bf16[2048,4]{0,1:T(4,128)(2,1)S(1)}, bf16[2048,4]{0,1:T(4,128)(2,1)}, u32[]{:S(2)}) copy-start(bf16[2048,4]{0,1:T(4,128)(2,1)} %param.32) | copy-start | bytes 49156
  47.0 41.8 %copy-start.7 = (bf16[2048,8]{0,1:T(8,128)(2,1)S(1)}, bf16[2048,8]{0,1:T(8,128)(2,1)}, u32[]{:S(2)}) copy-start(bf16[2048,8]{0,1:T(8,128)(2,1)} %param.33) | copy-start | bytes 98308
  47.0 42.1 %copy-start.4 = (s32[128,2]{0,1:T(2,128)S(1)}, s32[128,2]{0,1:T(2,128)}, u32[]{:S(2)}) copy-start(s32[128,2]{0,1:T(2,128)} %param.34) | copy-start | bytes 3076
  88.3 1.0 %copy-start.2 = (bf16[8,64,512]{2,1,0:T(8,128)(2,1)S(1)}, bf16[8,64,512]{2,1,0:T(8,128)(2,1)}, u32[]{:S(2)}) copy-start(bf16[8,64,512]{2,1,0:T(8,128)(2,1)} %get-tuple-element.13) | copy-start | bytes 1572868
  88.3 2.2 %copy-start.3 = (bf16[128,2048]{1,0:T(8,128)(2,1)S(1)}, bf16[128,2048]{1,0:T(8,128)(2,1)}, u32[]{:S(2)}) copy-start(bf16[128,2048]{1,0:T(8,128)(2,1)} %get-tuple-element.20) | copy-start | bytes 1572868

commit v4 on v3

--- a/solution.py
+++ b/solution.py
@@ -10,6 +10,7 @@
 
 HEAD_DIM = 64
 PAIR = 2 * HEAD_DIM
+BACK_LIMIT = 44 << 20
 HALF_EXP = math.exp(-0.5)
 GROUPS = 4
 
@@ -280,6 +281,8 @@
     own_sem,
     es,
     er,
+    zs,
+    zr,
     gs,
     gr,
     cs,
@@ -308,9 +311,42 @@
         peer = lax.rem(e + d, n_ep)
         return remote(cols_ref.at[peer], block(e, t), es.at[d], er.at[d], peer, t)
 
-    def ends_copy(d):
-        peer = lax.rem(e + d, n_ep)
-        return remote(ends_ref, every_ref.at[e], gs.at[d], gr.at[d], peer, t)
+    n_x = gs.shape[0]
+    n_z = n_ep // n_x
+    z, x = lax.div(e, n_x), lax.rem(e, n_x)
+
+    def up_copy(zz):
+        ref = every_ref.at[zz * n_x + x]
+        return remote(ref, ref, zs.at[zz], zr.at[zz], e + n_x, t)
+
+    def side_copy(zz, h):
+        ref = every_ref.at[zz * n_x + x]
+        peer = z * n_x + lax.rem(x + h, n_x)
+        return remote(ref, ref, gs.at[h, zz], gr.at[h, zz], peer, t)
+
+    def pass_ends(zz):
+        @pl.when(z + 1 < n_z)
+        def _():
+            up_copy(zz).start()
+
+        for h in range(1, n_x):
+            side_copy(zz, h).start()
+
+    def relay_ends(i):
+        @pl.when(z >= i)
+        def _():
+            up_copy(z - i).wait_recv()
+            pass_ends(z - i)
+
+    def close_ends(zz):
+        @pl.when(z >= zz)
+        def _():
+            @pl.when(z + 1 < n_z)
+            def _():
+                up_copy(zz).wait_send()
+
+            for h in range(1, n_x):
+                side_copy(zz, h).wait()
 
     def source(d):
         return lax.rem(e - d + n_ep, n_ep)
@@ -328,12 +364,12 @@
             block(source(d), index), block(source(d), index), fs.at[h, d], fr.at[h, d], e, other
         )
 
-    def every(first, body):
+    def every(first, body, last=n_ep):
         def run(d, carry):
             body(d)
             return carry
 
-        lax.fori_loop(first, n_ep, run, 0)
+        lax.fori_loop(first, last, run, 0)
 
     every(1, lambda d: ep_copy(d).start())
 
@@ -364,9 +400,11 @@
         ep_copy(d).wait_recv()
         share_out(d)
 
+    own_ends.start()
+    own_ends.wait()
+    pass_ends(z)
     every(1, arrived)
-    every(1, lambda d: ends_copy(d).start())
-    own_ends.start()
+    every(1, relay_ends, n_z)
 
     def pass_on(d):
         for h in range(1, n_y):
@@ -385,20 +423,26 @@
 
     def close_far(d):
         ep_copy(d).wait_send()
-        ends_copy(d).wait()
 
     every(1, close_far)
-    own_ends.wait()
+    every(0, close_ends, n_z)
 
 
 def return_kernel(
     piece_ref,
-    proj_ref,
+    every_ref,
+    local_ref,
+    reach_ref,
+    gate_in_ref,
+    gain_ref,
+    out_weight_ref,
     gate_hbm,
     up_hbm,
     down_hbm,
     home_ref,
     mixer_ref,
+    mixed_ref,
+    proj_ref,
     gate_ref,
     up_ref,
     down_ref,
@@ -574,6 +618,13 @@
         final_ref[s] = add_far(s)
         home_copy(k).start()
 
+    join_kernel("ep", every_ref, local_ref, reach_ref, gate_in_ref, gain_ref, mixed_ref)
+
+    def project(i):
+        at = pl.ds(pl.multiple_of(i * wide_model, wide_model), wide_model)
+        proj_ref[:, at] = bf(mm(mixed_ref[...], out_weight_ref[:, at]))
+
+    span(0, model // wide_model, project)
     meet()
     for q in range(2):
         for h in range(n_y):
@@ -609,12 +660,16 @@
     span(0, n_ep - 1, lambda k: home_copy(k).wait())
 
 
-def experts_and_back(piece, projected, gate_weight, up_weight, down_weight):
+def experts_and_back(
+    piece, everyone, local, reach, gate_input, gain, out_weight, gate_weight, up_weight, down_weight
+):
     n_ep, n_tp = lax.axis_size("ep"), lax.axis_size("tp")
     n_y = n_tp // 2
     capacity, model = piece.shape[1:]
     units = gate_weight.shape[2]
-    share, rows = model // n_tp, projected.shape[0] // n_tp
+    share, rows = model // n_tp, local.shape[0] // n_tp
+    width = local.shape[1]
+    out_weight = jnp.pad(out_weight, ((0, width - out_weight.shape[0]), (0, 0)))
     many, few = pltpu.SemaphoreType.DMA((n_ep, n_y)), pltpu.SemaphoreType.DMA((2, n_y))
     one = pltpu.SemaphoreType.DMA((n_ep,))
 
@@ -628,9 +683,11 @@
             jax.ShapeDtypeStruct((n_ep, capacity, share), jnp.bfloat16),
             jax.ShapeDtypeStruct((rows, model), jnp.bfloat16),
         ),
-        in_specs=[in_vmem] * 2 + [pl.BlockSpec(memory_space=pl.ANY)] * 3,
+        in_specs=[in_vmem] * 7 + [pl.BlockSpec(memory_space=pltpu.HBM)] * 3,
         out_specs=[in_vmem] * 2,
         scratch_shapes=[
+            held(*local.shape),
+            held(local.shape[0], model),
             held(model, units),
             held(model, units),
             held(units, model),
@@ -646,8 +703,21 @@
         + [many] * 4
         + [one] * 2
         + [few] * 4,
-        compiler_params=pltpu.CompilerParams(collective_id=1, has_side_effects=True),
-    )(piece, projected, gate_weight, up_weight, down_weight)
+        compiler_params=pltpu.CompilerParams(
+            collective_id=1, has_side_effects=True, vmem_limit_bytes=BACK_LIMIT
+        ),
+    )(
+        piece,
+        everyone,
+        local,
+        reach,
+        gate_input,
+        gain,
+        out_weight,
+        gate_weight,
+        up_weight,
+        down_weight,
+    )
 
 
 def scan_and_dispatch(
@@ -674,6 +744,9 @@
     group = 4 if blocks % 4 == 0 else 1
     n_ep, n_tp = lax.axis_size("ep"), lax.axis_size("tp")
     n_y = n_tp // 2
+    n_x = 1
+    while 4 * n_x * n_x <= n_ep:
+        n_x = 2 * n_x
     capacity, share = own_columns.shape[1:]
     ends = (pairs * 2 * HEAD_DIM, PAIR)
     one, many = pltpu.SemaphoreType.DMA((n_ep,)), pltpu.SemaphoreType.DMA((n_y, n_ep))
@@ -692,9 +765,14 @@
             pltpu.VMEM(ends, jnp.bfloat16),
             pltpu.SemaphoreType.DMA((2,)),
         ]
-        + [one] * 6
+        + [one] * 2
+        + [pltpu.SemaphoreType.DMA((n_ep // n_x,))] * 2
+        + [pltpu.SemaphoreType.DMA((n_x, n_ep // n_x))] * 2
+        + [one] * 2
         + [many] * 4,
-        compiler_params=pltpu.CompilerParams(collective_id=0, has_side_effects=True),
+        compiler_params=pltpu.CompilerParams(
+            collective_id=0, has_side_effects=True, vmem_limit_bytes=16 << 20
+        ),
     )(
         filled(receptance),
         filled(key_matrix),
@@ -708,22 +786,6 @@
     )
     gate_input, gain = filled(output_gate_input), filled(head_norm_gain[None])
     return local, reach, piece, everyone, gate_input, gain
-
-
-def mixer_finish(everyone, local, reach, gate_input, gain, mixer_output_weight):
-    positions, width = local.shape
-    own_width = mixer_output_weight.shape[0]
-    mixed_hidden = pl.pallas_call(
-        functools.partial(join_kernel, "ep"),
-        out_shape=jax.ShapeDtypeStruct((positions, width), jnp.bfloat16),
-        cost_estimate=pl.CostEstimate(
-            flops=6000 * positions * width, bytes_accessed=16 * positions * width, transcendentals=0
-        ),
-    )(everyone, local, reach, gate_input, gain)
-    mixed_hidden = mixed_hidden[:, :own_width]
-    return jnp.dot(mixed_hidden, mixer_output_weight, preferred_element_type=jnp.float32).astype(
-        jnp.bfloat16
-    )
 
 
 def expert_route(
@@ -827,9 +889,17 @@
         extra_head_log_decay,
         head_norm_gain,
     )
-    projected = mixer_finish(everyone, local_read, reach, gate_input, gain, mixer_output_weight)
     homebound, token_mixer_output = experts_and_back(
-        piece, projected, expert_gate_weight, expert_up_weight, expert_down_weight
+        piece,
+        everyone,
+        local_read,
+        reach,
+        gate_input,
+        gain,
+        mixer_output_weight,
+        expert_gate_weight,
+        expert_up_weight,
+        expert_down_weight,
     )
     return (token_mixer_output, expert_combine(homebound, combine_matrix))
 

time: 91.6 us -> 78.9 us (0.86)
  Pallas kernels: 76.8 us -> 63.7 us
  local copies, waits for them, and re-layouts: 4.3 us -> 5.94 us
  matrix products: 6.54 us -> 4.94 us
    pallas_call x1, Pallas kernels: 32.5 us -> 26.2 us  [scan_and_dispatch(): pl.pallas_call(functools.partial(dispatch_kernel, group), out_shape=(jax....]
    pallas_call x1, Pallas kernels: 41.3 us -> 37.5 us  [experts_and_back(): pl.pallas_call(return_kernel, out_shape=(jax.ShapeDtypeStruct((n_ep, capa...]
    dot_general x1 -> x0, matrix products: 2.96 us -> none  [mixer_finish(): jnp.dot(mixed_hidden, mixer_output_weight, preferred_element_type=jnp.flo...]
    pallas_call x1 -> x0, Pallas kernels: 2.93 us -> none  [mixer_finish(): pl.pallas_call(functools.partial(join_kernel, 'ep'), out_shape=jax.ShapeD...]
    unnamed x21 -> x37, local copies, waits for them, and re-layouts: 2.73 us -> 4.13 us
    dot_general x1, matrix products: 1.83 us -> 3.18 us  [expert_route(): jnp.dot(dispatch_matrix, normed_input, preferred_element_type=jnp.float32)]
where the time goes in v4:
time: 78.9 us; the launch traced here: 78.4 us
  Pallas kernels  63.7 us (81%)
  local copies, waits for them, and re-layouts  5.94 us (8%)
  matrix products  4.94 us (6%)
  other arithmetic  2.87 us (4%)
  between operations  0.94 us (1%)
    pallas_call x1, Pallas kernels, experts_and_back(): pl.pallas_call(return_kernel, out_shape=(jax.ShapeDtypeStruct((n_ep, capa...  37.5 us
    pallas_call x1, Pallas kernels, scan_and_dispatch(): pl.pallas_call(functools.partial(dispatch_kernel, group), out_shape=(jax....  26.2 us
    unnamed x37, local copies, waits for them, and re-layouts  4.13 us
    dot_general x1, matrix products, expert_route(): jnp.dot(dispatch_matrix, normed_input, preferred_element_type=jnp.float32)  3.18 us

profile of v4, /device:TPU:0, one launch (start us, length us, event | category | flops | bytes accessed | tf_op | source)
XLA Modules:
  0.0 78.4 jit_solution(17650499224229228079)
XLA Ops:
  0.6 0.0 copy-start
  0.6 0.0 copy-start.15
  0.7 0.0 copy-start.9
  0.7 0.0 copy-start.10
  0.7 0.0 copy-start.4
  0.7 0.0 copy-start.5
  0.7 0.0 copy-start.6
  0.7 0.0 copy-start.7
  0.7 0.0 copy-start.8
  0.7 0.0 copy-start.11
  0.7 0.0 copy-start.3
  0.7 0.0 copy-start.2
  0.8 0.9 %copy.42 = s32[128,2]{1,0:T(8,128)S(1)} copy(s32[128,2]{0,1:T(2,128)} %param.34) | data formatting | bytes 2048 | tf_op args[15]
  1.7 0.1 eq.64
  1.8 0.6 reduce-window.6
  2.4 0.2 slice_reduce_fusion
  2.7 0.1 eq.60
  2.8 0.1 fusion.5
  2.9 0.1 reduce_sum.57
  3.1 0.1 copy.44
  3.1 0.7 and_select_fusion
  3.8 0.1 fusion.3
  3.9 1.2 %fusion = f32[128]{0:T(128)S(1)} fusion(bf16[128,2048]{1,0:T(8,128)(2,1)} %param.30), kind=kLoop, calls=%fused_computation.5 | loop fusion | flops 786304 | bytes 524800 | tf_op jit(solution)/shard_map/reduce_sum | solution.py:807
  5.1 3.2 %convolution_convert_fusion = bf16[512,2048]{1,0:T(8,128)(2,1)} fusion(pred[512,128]{1,0:T(8,128)(4,1)S(1)} %fusion.3, bf16[128,2048]{1,0:T(8,128)(2,1)} %param.30, f32[2048]{0:T(1024)} %param.31, f32[128]{0:T(128)S(1)} %add_rsqrt_fusion), kind=kOutput, calls=%fused_computation | convolution fusion | flops 270532608 | bytes 2695680 | tf_op jit(solution)/shard_map/dot_general | solution.py:832
  8.3 1.1 %constant_dynamic-slice_fusion.cols_ref = bf16[8,64,512]{2,1,0:T(8,128)(2,1)S(1)} fusion(bf16[8,64,2048]{2,1,0:T(8,128)(2,1)} %bitcast.22, s32[]{:T(128)S(6)} %select_n.20), kind=kLoop, calls=%fused_computation.30 | loop fusion | bytes 1048580 | tf_op jit(solution)/shard_map/dynamic_slice | solution.py:837
  9.4 0.0 copy-done.15
  9.4 0.1 copy.45.extra_ref
  9.6 0.0 copy-done.9
  9.6 0.0 copy-done.10
  9.6 0.0 copy-done.4
  9.6 0.0 copy-done.5
  9.6 0.0 copy-done.6
  9.6 0.0 copy-done.7
  9.6 0.0 copy-done.8
  9.7 26.2 %shard_map.194 = (f32[512,256]{1,0:T(8,128)S(1)}, bf16[512,256]{1,0:T(8,128)(2,1)S(1)}, bf16[8,64,2048]{2,1,0:T(8,128)(2,1)S(1)}, bf16[8,256,128]{2,1,0:T(8,128)(2,1)S(1)}) custom-call(bf16[512,256]{1,0:T(8,128)(2,1)S(1)} %copy-done.4, bf16[512,256]{1,0:T(8,128)(2,1)S(1)} %copy-done.5, bf16[512,256]{1,0:T(8,128)(2,1)S(1)} %copy-done.6, ...), custom_call_target="tpu_custom_call" | custom-call | tf_op jit(solution)/shard_map/pallas_call | solution.py:753
  35.9 0.0 copy-done.11
  35.9 0.0 copy-done.3
  35.9 0.0 copy-done.2
  35.9 0.0 copy-start.1
  35.9 2.2 %copy-done.1 = bf16[1,2048,1024]{2,1,0:T(8,128)(2,1)S(1)} copy-done((bf16[1,2048,1024]{2,1,0:T(8,128)(2,1)S(1)}, bf16[1,2048,1024]{2,1,0:T(8,128)(2,1)}, u32[]{:S(2)}) %copy-start.1) | copy-done | bytes 4194328
  38.1 37.5 %shard_map.195 = (bf16[8,64,512]{2,1,0:T(8,128)(2,1)S(1)}, bf16[128,2048]{1,0:T(8,128)(2,1)S(1)}) custom-call(bf16[8,64,2048]{2,1,0:T(8,128)(2,1)S(1)} %get-tuple-element.8.piece_ref, bf16[8,256,128]{2,1,0:T(8,128)(2,1)S(1)} %get-tuple-element.9.every_ref, f32[512,256]{1,0:T(8,128)S(1)} %get-tuple-element.10.local_ref, ...), custom_call_target="tpu_custom_call" | custom-call | tf_op jit(solution)/shard_map/pallas_call | solution.py:680
  75.6 0.3 fusion.11
  76.0 0.0 copy-done
  76.0 0.3 fusion.7
  76.3 0.0 copy-done.13
  76.4 0.1 select_reduce_fusion
  76.5 1.1 %convolution_convert_fusion.1 = bf16[128,512]{1,0:T(8,128)(2,1)} fusion(f32[512,128]{1,0:T(8,128)S(1)} %select_reduce_fusion, bf16[512,512]{1,0:T(8,128)(2,1)S(1)} %bitcast.18), kind=kOutput, calls=%fused_computation.3 | convolution fusion | flops 402718720 | bytes 917504 | tf_op jit(solution)/shard_map/dot_general | solution.py:845
  77.6 0.8 %copy.47 = bf16[128,2048]{1,0:T(8,128)(2,1)} copy(bf16[128,2048]{1,0:T(8,128)(2,1)S(1)} %get-tuple-element.20) | data formatting | bytes 1048576
  (16 shorter events, 0.2 us)
Async XLA Ops:
  0.6 75.4 %copy-start = (bf16[2048,8]{0,1:T(8,128)(2,1)S(1)}, bf16[2048,8]{0,1:T(8,128)(2,1)}, u32[]{:S(2)}) copy-start(bf16[2048,8]{0,1:T(8,128)(2,1)} %param.33) | copy-start | bytes 98308
  0.6 8.8 %copy-start.15 = (f32[512,4]{0,1:T(4,128)S(1)}, f32[512,4]{0,1:T(4,128)}, u32[]{:S(2)}) copy-start(f32[512,4]{0,1:T(4,128)} %param.27) | copy-start | bytes 24580
  0.7 8.9 %copy-start.9 = (f32[256]{0:T(256)S(1)}, f32[256]{0:T(256)}, u32[]{:S(2)}) copy-start(f32[256]{0:T(256)} %param.25) | copy-start | bytes 3076
  0.7 8.9 %copy-start.10 = (f32[256]{0:T(256)S(1)}, f32[256]{0:T(256)}, u32[]{:S(2)}) copy-start(f32[256]{0:T(256)} %param.26) | copy-start | bytes 3076
  0.7 8.9 %copy-start.4 = (bf16[512,256]{1,0:T(8,128)(2,1)S(1)}, bf16[512,256]{1,0:T(8,128)(2,1)}, u32[]{:S(2)}) copy-start(bf16[512,256]{1,0:T(8,128)(2,1)} %r_ref.1) | copy-start | bytes 786436
  0.7 8.9 %copy-start.5 = (bf16[512,256]{1,0:T(8,128)(2,1)S(1)}, bf16[512,256]{1,0:T(8,128)(2,1)}, u32[]{:S(2)}) copy-start(bf16[512,256]{1,0:T(8,128)(2,1)} %k_ref.1) | copy-start | bytes 786436
  0.7 8.9 %copy-start.6 = (bf16[512,256]{1,0:T(8,128)(2,1)S(1)}, bf16[512,256]{1,0:T(8,128)(2,1)}, u32[]{:S(2)}) copy-start(bf16[512,256]{1,0:T(8,128)(2,1)} %v_ref.1) | copy-start | bytes 786436
  0.7 8.9 %copy-start.7 = (bf16[512,256]{1,0:T(8,128)(2,1)S(1)}, bf16[512,256]{1,0:T(8,128)(2,1)}, u32[]{:S(2)}) copy-start(bf16[512,256]{1,0:T(8,128)(2,1)} %d_ref.1) | copy-start | bytes 786436
  0.7 8.9 %copy-start.8 = (bf16[512,256]{1,0:T(8,128)(2,1)S(1)}, bf16[512,256]{1,0:T(8,128)(2,1)}, u32[]{:S(2)}) copy-start(bf16[512,256]{1,0:T(8,128)(2,1)} %a_ref.1) | copy-start | bytes 786436
  0.7 35.1 %copy-start.11 = (f32[256]{0:T(256)S(1)}, f32[256]{0:T(256)}, u32[]{:S(2)}) copy-start(f32[256]{0:T(256)} %param.28) | copy-start | bytes 3076
  0.7 35.1 %copy-start.3 = (bf16[512,256]{1,0:T(8,128)(2,1)S(1)}, bf16[512,256]{1,0:T(8,128)(2,1)}, u32[]{:S(2)}) copy-start(bf16[512,256]{1,0:T(8,128)(2,1)} %gate_in_ref.1) | copy-start | bytes 786436
  0.7 35.1 %copy-start.2 = (bf16[256,2048]{1,0:T(8,128)(2,1)S(1)}, bf16[256,2048]{1,0:T(8,128)(2,1)}, u32[]{:S(2)}) copy-start(bf16[256,2048]{1,0:T(8,128)(2,1)} %out_weight_ref.1) | copy-start | bytes 3145732
  35.9 2.2 %copy-start.1 = (bf16[1,2048,1024]{2,1,0:T(8,128)(2,1)S(1)}, bf16[1,2048,1024]{2,1,0:T(8,128)(2,1)}, u32[]{:S(2)}) copy-start(bf16[1,2048,1024]{2,1,0:T(8,128)(2,1)} %gate_hbm.1) | copy-start | bytes 12582916
  38.1 37.5 %copy-start.12 = (bf16[128,2048]{1,0:T(8,128)(2,1)S(1)}, bf16[128,2048]{1,0:T(8,128)(2,1)}, u32[]{:S(2)}) copy-start(bf16[128,2048]{1,0:T(8,128)(2,1)} %param.30) | copy-start | bytes 1572868
  38.1 37.5 %copy-start.14 = (f32[2048]{0:T(1024)S(1)}, f32[2048]{0:T(1024)}, u32[]{:S(2)}) copy-start(f32[2048]{0:T(1024)} %param.31) | copy-start | bytes 24580
  38.1 37.5 %copy-start.16 = (bf16[2048,4]{0,1:T(4,128)(2,1)S(1)}, bf16[2048,4]{0,1:T(4,128)(2,1)}, u32[]{:S(2)}) copy-start(bf16[2048,4]{0,1:T(4,128)(2,1)} %param.32) | copy-start | bytes 49156
  38.1 38.2 %copy-start.13 = (s32[128,2]{0,1:T(2,128)S(1)}, s32[128,2]{0,1:T(2,128)}, u32[]{:S(2)}) copy-start(s32[128,2]{0,1:T(2,128)} %param.34) | copy-start | bytes 3076

commit v5 on v4

--- a/solution.py
+++ b/solution.py
@@ -10,7 +10,7 @@
 
 HEAD_DIM = 64
 PAIR = 2 * HEAD_DIM
-BACK_LIMIT = 44 << 20
+BACK_LIMIT = 32 << 20
 HALF_EXP = math.exp(-0.5)
 GROUPS = 4
 
@@ -773,6 +773,11 @@
         compiler_params=pltpu.CompilerParams(
             collective_id=0, has_side_effects=True, vmem_limit_bytes=16 << 20
         ),
+        cost_estimate=pl.CostEstimate(
+            flops=200000 * positions * width,
+            bytes_accessed=16 * positions * width,
+            transcendentals=0,
+        ),
     )(
         filled(receptance),
         filled(key_matrix),

time: 78.9 us -> 78.3 us (level)
  local copies, waits for them, and re-layouts: 5.94 us -> 3.74 us
  Pallas kernels: 63.7 us -> 65.3 us
    unnamed x37 -> x41, local copies, waits for them, and re-layouts: 4.13 us -> 1.93 us
    pallas_call x1, Pallas kernels: 37.5 us -> 39.1 us  [experts_and_back(): pl.pallas_call(return_kernel, out_shape=(jax.ShapeDtypeStruct((n_ep, capa...]
where the time goes in v5:
time: 78.3 us; the launch traced here: 77.8 us
  Pallas kernels  65.3 us (83%)
  matrix products  4.91 us (6%)
  local copies, waits for them, and re-layouts  3.74 us (5%)
  other arithmetic  2.87 us (4%)
  between operations  1.01 us (1%)
    pallas_call x1, Pallas kernels, experts_and_back(): pl.pallas_call(return_kernel, out_shape=(jax.ShapeDtypeStruct((n_ep, capa...  39.1 us
    pallas_call x1, Pallas kernels, scan_and_dispatch(): pl.pallas_call(functools.partial(dispatch_kernel, group), out_shape=(jax....  26.2 us
    dot_general x1, matrix products, expert_route(): jnp.dot(dispatch_matrix, normed_input, preferred_element_type=jnp.float32)  3.18 us
    unnamed x41, local copies, waits for them, and re-layouts  1.93 us

profile of v5, /device:TPU:0, one launch (start us, length us, event | category | flops | bytes accessed | tf_op | source)
XLA Modules:
  0.0 77.8 jit_solution(5647268120862471368)
XLA Ops:
  0.6 0.0 copy-start
  0.6 0.0 copy-start.17
  0.7 0.0 copy-start.12
  0.7 0.0 copy-start.13
  0.7 0.0 copy-start.7
  0.7 0.0 copy-start.8
  0.7 0.0 copy-start.9
  0.7 0.0 copy-start.10
  0.7 0.0 copy-start.11
  0.7 0.9 %copy.42 = s32[128,2]{1,0:T(8,128)S(1)} copy(s32[128,2]{0,1:T(2,128)} %param.34) | data formatting | bytes 2048 | tf_op args[15]
  1.6 0.1 eq.64
  1.8 0.6 reduce-window.6
  2.4 0.2 slice_reduce_fusion
  2.6 0.1 eq.60
  2.8 0.1 fusion.5
  2.8 0.1 reduce_sum.57
  3.0 0.1 copy.44
  3.1 0.7 and_select_fusion
  3.8 0.1 fusion.3
  3.8 1.2 %fusion = f32[128]{0:T(128)S(1)} fusion(bf16[128,2048]{1,0:T(8,128)(2,1)} %param.30), kind=kLoop, calls=%fused_computation.5 | loop fusion | flops 786304 | bytes 524800 | tf_op jit(solution)/shard_map/reduce_sum | solution.py:812
  5.1 3.2 %convolution_convert_fusion = bf16[512,2048]{1,0:T(8,128)(2,1)} fusion(pred[512,128]{1,0:T(8,128)(4,1)S(1)} %fusion.3, bf16[128,2048]{1,0:T(8,128)(2,1)} %param.30, f32[2048]{0:T(1024)} %param.31, f32[128]{0:T(128)S(1)} %add_rsqrt_fusion), kind=kOutput, calls=%fused_computation | convolution fusion | flops 270532608 | bytes 2695680 | tf_op jit(solution)/shard_map/dot_general | solution.py:837
  8.2 1.1 %constant_dynamic-slice_fusion.cols_ref = bf16[8,64,512]{2,1,0:T(8,128)(2,1)S(1)} fusion(bf16[8,64,2048]{2,1,0:T(8,128)(2,1)} %bitcast.22, s32[]{:T(128)S(6)} %select_n.20), kind=kLoop, calls=%fused_computation.30 | loop fusion | bytes 1048580 | tf_op jit(solution)/shard_map/dynamic_slice | solution.py:842
  9.3 0.0 copy-done.17
  9.4 0.1 copy.45.extra_ref
  9.5 0.0 copy-done.12
  9.5 0.0 copy-done.13
  9.5 0.0 copy-done.7
  9.5 0.0 copy-done.8
  9.5 0.0 copy-done.9
  9.6 0.0 copy-done.10
  9.6 0.0 copy-done.11
  9.6 0.0 copy-start.1
  9.6 0.0 copy-start.2
  9.6 0.0 copy-start.3
  9.6 0.0 copy-start.4
  9.6 0.0 copy-start.5
  9.6 0.0 copy-start.6
  9.6 26.2 %shard_map.194 = (f32[512,256]{1,0:T(8,128)S(1)}, bf16[512,256]{1,0:T(8,128)(2,1)S(1)}, bf16[8,64,2048]{2,1,0:T(8,128)(2,1)S(1)}, bf16[8,256,128]{2,1,0:T(8,128)(2,1)S(1)}) custom-call(bf16[512,256]{1,0:T(8,128)(2,1)S(1)} %copy-done.7, bf16[512,256]{1,0:T(8,128)(2,1)S(1)} %copy-done.8, bf16[512,256]{1,0:T(8,128)(2,1)S(1)} %copy-done.9, ...), custom_call_target="tpu_custom_call" | custom-call | flops 26214400000 | bytes 2097152 | tf_op jit(solution)/shard_map/pallas_call | solution.py:753
  35.9 0.0 copy-start.14
  35.9 0.0 copy-start.16
  36.0 0.0 copy-start.18
  36.0 0.0 copy-start.15
  36.0 39.1 %shard_map.195 = (bf16[8,64,512]{2,1,0:T(8,128)(2,1)S(1)}, bf16[128,2048]{1,0:T(8,128)(2,1)S(1)}) custom-call(bf16[8,64,2048]{2,1,0:T(8,128)(2,1)S(1)} %get-tuple-element.8.piece_ref, bf16[8,256,128]{2,1,0:T(8,128)(2,1)S(1)} %get-tuple-element.9.every_ref, f32[512,256]{1,0:T(8,128)S(1)} %get-tuple-element.10.local_ref, ...), custom_call_target="tpu_custom_call" | custom-call | tf_op jit(solution)/shard_map/pallas_call | solution.py:680
  75.1 0.3 fusion.11
  75.5 0.3 fusion.7
  75.8 0.1 select_reduce_fusion
  75.9 1.1 %convolution_convert_fusion.1 = bf16[128,512]{1,0:T(8,128)(2,1)} fusion(f32[512,128]{1,0:T(8,128)S(1)} %select_reduce_fusion, bf16[512,512]{1,0:T(8,128)(2,1)S(1)} %bitcast.18), kind=kOutput, calls=%fused_computation.3 | convolution fusion | flops 402718720 | bytes 917504 | tf_op jit(solution)/shard_map/dot_general | solution.py:850
  77.0 0.8 %copy.47 = bf16[128,2048]{1,0:T(8,128)(2,1)} copy(bf16[128,2048]{1,0:T(8,128)(2,1)S(1)} %get-tuple-element.20) | data formatting | bytes 1048576
  (20 shorter events, 0.2 us)
Async XLA Ops:
  0.6 74.8 %copy-start = (bf16[2048,8]{0,1:T(8,128)(2,1)S(1)}, bf16[2048,8]{0,1:T(8,128)(2,1)}, u32[]{:S(2)}) copy-start(bf16[2048,8]{0,1:T(8,128)(2,1)} %param.33) | copy-start | bytes 98308
  0.6 8.7 %copy-start.17 = (f32[512,4]{0,1:T(4,128)S(1)}, f32[512,4]{0,1:T(4,128)}, u32[]{:S(2)}) copy-start(f32[512,4]{0,1:T(4,128)} %param.27) | copy-start | bytes 24580
  0.7 8.8 %copy-start.12 = (f32[256]{0:T(256)S(1)}, f32[256]{0:T(256)}, u32[]{:S(2)}) copy-start(f32[256]{0:T(256)} %param.25) | copy-start | bytes 3076
  0.7 8.8 %copy-start.13 = (f32[256]{0:T(256)S(1)}, f32[256]{0:T(256)}, u32[]{:S(2)}) copy-start(f32[256]{0:T(256)} %param.26) | copy-start | bytes 3076
  0.7 8.8 %copy-start.7 = (bf16[512,256]{1,0:T(8,128)(2,1)S(1)}, bf16[512,256]{1,0:T(8,128)(2,1)}, u32[]{:S(2)}) copy-start(bf16[512,256]{1,0:T(8,128)(2,1)} %r_ref.1) | copy-start | bytes 786436
  0.7 8.8 %copy-start.8 = (bf16[512,256]{1,0:T(8,128)(2,1)S(1)}, bf16[512,256]{1,0:T(8,128)(2,1)}, u32[]{:S(2)}) copy-start(bf16[512,256]{1,0:T(8,128)(2,1)} %k_ref.1) | copy-start | bytes 786436
  0.7 8.8 %copy-start.9 = (bf16[512,256]{1,0:T(8,128)(2,1)S(1)}, bf16[512,256]{1,0:T(8,128)(2,1)}, u32[]{:S(2)}) copy-start(bf16[512,256]{1,0:T(8,128)(2,1)} %v_ref.1) | copy-start | bytes 786436
  0.7 8.8 %copy-start.10 = (bf16[512,256]{1,0:T(8,128)(2,1)S(1)}, bf16[512,256]{1,0:T(8,128)(2,1)}, u32[]{:S(2)}) copy-start(bf16[512,256]{1,0:T(8,128)(2,1)} %d_ref.1) | copy-start | bytes 786436
  0.7 8.8 %copy-start.11 = (bf16[512,256]{1,0:T(8,128)(2,1)S(1)}, bf16[512,256]{1,0:T(8,128)(2,1)}, u32[]{:S(2)}) copy-start(bf16[512,256]{1,0:T(8,128)(2,1)} %a_ref.1) | copy-start | bytes 786436
  9.6 26.3 %copy-start.1 = (bf16[1,2048,1024]{2,1,0:T(8,128)(2,1)S(1)}, bf16[1,2048,1024]{2,1,0:T(8,128)(2,1)}, u32[]{:S(2)}) copy-start(bf16[1,2048,1024]{2,1,0:T(8,128)(2,1)} %gate_hbm.1) | copy-start | bytes 12582916
  9.6 26.3 %copy-start.2 = (bf16[1,2048,1024]{2,1,0:T(8,128)(2,1)S(1)}, bf16[1,2048,1024]{2,1,0:T(8,128)(2,1)}, u32[]{:S(2)}) copy-start(bf16[1,2048,1024]{2,1,0:T(8,128)(2,1)} %up_hbm.1) | copy-start | bytes 12582916
  9.6 26.3 %copy-start.3 = (bf16[1,1024,2048]{2,1,0:T(8,128)(2,1)S(1)}, bf16[1,1024,2048]{2,1,0:T(8,128)(2,1)}, u32[]{:S(2)}) copy-start(bf16[1,1024,2048]{2,1,0:T(8,128)(2,1)} %down_hbm.1) | copy-start | bytes 12582916
  9.6 26.3 %copy-start.4 = (bf16[256,2048]{1,0:T(8,128)(2,1)S(1)}, bf16[256,2048]{1,0:T(8,128)(2,1)}, u32[]{:S(2)}) copy-start(bf16[256,2048]{1,0:T(8,128)(2,1)} %out_weight_ref.1) | copy-start | bytes 3145732
  9.6 26.3 %copy-start.5 = (bf16[512,256]{1,0:T(8,128)(2,1)S(1)}, bf16[512,256]{1,0:T(8,128)(2,1)}, u32[]{:S(2)}) copy-start(bf16[512,256]{1,0:T(8,128)(2,1)} %gate_in_ref.1) | copy-start | bytes 786436
  9.6 26.3 %copy-start.6 = (f32[256]{0:T(256)S(1)}, f32[256]{0:T(256)}, u32[]{:S(2)}) copy-start(f32[256]{0:T(256)} %param.28) | copy-start | bytes 3076
  35.9 39.1 %copy-start.14 = (bf16[128,2048]{1,0:T(8,128)(2,1)S(1)}, bf16[128,2048]{1,0:T(8,128)(2,1)}, u32[]{:S(2)}) copy-start(bf16[128,2048]{1,0:T(8,128)(2,1)} %param.30) | copy-start | bytes 1572868
  35.9 39.1 %copy-start.16 = (f32[2048]{0:T(1024)S(1)}, f32[2048]{0:T(1024)}, u32[]{:S(2)}) copy-start(f32[2048]{0:T(1024)} %param.31) | copy-start | bytes 24580
  36.0 39.1 %copy-start.18 = (bf16[2048,4]{0,1:T(4,128)(2,1)S(1)}, bf16[2048,4]{0,1:T(4,128)(2,1)}, u32[]{:S(2)}) copy-start(bf16[2048,4]{0,1:T(4,128)(2,1)} %param.32) | copy-start | bytes 49156
  36.0 39.8 %copy-start.15 = (s32[128,2]{0,1:T(2,128)S(1)}, s32[128,2]{0,1:T(2,128)}, u32[]{:S(2)}) copy-start(s32[128,2]{0,1:T(2,128)} %param.34) | copy-start | bytes 3076
